TPU v7x, 32 devices: a whole 2x2x4 slice. The times are simulated.
32 devices in a mesh: sp: 8 (over z, y), tp: 4 (over x, core).
Axes of the slice: x: 2, y: 2, z: 4, core: 2. Of those that a mesh axis runs over, the one named last changes fastest.
Arguments:
- mixer_output_stream: bfloat16 [1024, 2048], P('sp', 'tp'), may hold values from -6 to 6
- layer_output_gradient: bfloat16 [1024, 2048], P('sp', 'tp'), may hold values from -2.5 to 2.5
- routes: int32 [1024, 2], P('sp'), may hold values from 0 to 7, all different within a row; in each aligned block of 128 rows (0 to 127, 128 to 255, ...) at most 48 rows name the same one
- expert_combine_weight: float32 [1024, 2], P('sp'), may hold values from 0.2 to 1
- expert_gate_weight: bfloat16 [8, 2048, 3584], P('sp', None, 'tp'), may hold values from -0.125 to 0.125
- expert_up_weight: bfloat16 [8, 2048, 3584], P('sp', None, 'tp'), may hold values from -0.125 to 0.125
- expert_down_weight: bfloat16 [8, 3584, 2048], P('sp', 'tp'), may hold values from -0.09375 to 0.09375
- head_mixer_input: bfloat16 [1024, 4096], P('sp', 'tp'), may hold values from -6 to 6
- head_step_size: float32 [1024, 64], P('sp', 'tp'), may hold values from 0.25 to 4
- head_decay_rate: float32 [64], P('tp'), may hold values from 0 to 1
- extra_log_decay: float32 [1024, 64], P('sp', 'tp'), may hold values from -3 to 0
- state_entering_span: float32 [64, 64, 128], P('tp'), may hold values from -48 to 48
- state_input_vectors: bfloat16 [1024, 1024], P('sp', 'tp'), may hold values from -1.75 to 1.75
- state_readout_vectors: bfloat16 [1024, 1024], P('sp', 'tp'), may hold values from -1.75 to 1.75
- gate_preactivation: bfloat16 [1024, 4096], P('sp', 'tp'), may hold values from -6 to 6
- group_norm_scale: float32 [4096], P('tp'), may hold values from 0.1 to 1.9
- mixer_output_weight: bfloat16 [4096, 2048], P('tp', 'sp'), may hold values from -0.09375 to 0.09375
Outputs:
- grad_gate: bfloat16 [8, 2048, 3584], P('sp', None, 'tp')
- grad_up: bfloat16 [8, 2048, 3584], P('sp', None, 'tp')
- grad_down: bfloat16 [8, 3584, 2048], P('sp', 'tp')
- grad_out_proj: float32 [4096, 2048], P('tp', 'sp')
- grad_input: bfloat16 [1024, 4096], P('sp', 'tp')
- grad_step: float32 [1024, 64], P('sp', 'tp')
- grad_state_in: bfloat16 [1024, 1024], P('sp', 'tp')
- grad_read_out: bfloat16 [1024, 1024], P('sp', 'tp')
- grad_gate_in: bfloat16 [1024, 4096], P('sp', 'tp')
Inputs may be any that keep to these rules, and one draw needn't show every extreme that they name: `routes`: the two experts of a token differ. In each aligned block of 128 rows no expert is named more than 48 times, and in every draw some expert is named exactly 48 times in some block.
All inputs are finite; a program needn't handle non-finite values.
Results may differ from a plain program's by a relative error of at most 0.02.
Values may be sent and summed in bfloat16 or wider, within the bound.
A program may use at most 128 MiB of HBM per device.

v0:
```python
import jax
import jax.numpy as jnp
from jax import lax
from jax.sharding import PartitionSpec as P

HDIM = 64
STATE = 128
BLK = 128


norm_eps = 1e-05
exact_mode = lax.Precision.HIGH


def span_rows(x, axis):
    return lax.all_to_all(
        x.astype(jnp.bfloat16), axis, split_axis=0, concat_axis=0, tiled=True
    ).astype(jnp.float32)


def state_before(state, decay, first_state, axis):
    count, here = (lax.axis_size(axis), lax.axis_index(axis))
    width = state.shape[-1]
    rows = state.shape[0] * state.shape[1]
    per = rows // count
    row_decay = jnp.repeat(decay, state.shape[1]).reshape(count, per)
    lines = -(-per // width)
    row_decay = jnp.pad(row_decay, ((0, 0), (0, lines * width - per)))
    packed = jnp.concatenate(
        [state.reshape(count, per, width), row_decay.reshape(count, lines, width)], axis=1
    )
    arrived = span_rows(packed, axis)
    decays = arrived[:, per:].reshape(count, lines * width)[:, :per, None]
    running = lax.dynamic_slice_in_dim(first_state.reshape(rows, width), here * per, per, 0)
    before = []
    for k in range(count):
        before.append(running)
        running = decays[k] * running + arrived[k, :per]
    return (span_rows(jnp.stack(before), axis).reshape(state.shape), decays)


def gradient_after(reached, decays, axis):
    count = lax.axis_size(axis)
    width = reached.shape[-1]
    arrived = span_rows(reached.reshape(count, -1, width), axis)
    running = jnp.zeros_like(arrived[0])
    after = []
    for k in reversed(range(count)):
        after.append(running)
        running = decays[k] * running + arrived[k]
    return span_rows(jnp.stack(after[::-1]), axis).reshape(reached.shape)


def span_local_scan(
    input_heads,
    time_step,
    decay_speed,
    sudden_decay,
    input_vector_groups,
    readout_groups,
    starting_state,
):
    length, head_count, head_size = input_heads.shape
    groups, state_size = (input_vector_groups.shape[1], input_vector_groups.shape[2])
    per_group = head_count // groups
    block_count = length // BLK
    log_decay_total = sudden_decay - time_step * decay_speed[None, :]
    scaled = (input_heads * time_step[:, :, None]).reshape(
        block_count, BLK, groups, per_group, head_size
    )
    log_decay_total = log_decay_total.reshape(block_count, BLK, groups, per_group)
    b_rows = input_vector_groups.reshape(block_count, BLK, groups, state_size)
    c_rows = readout_groups.reshape(block_count, BLK, groups, state_size)
    cumulative = jnp.cumsum(log_decay_total, axis=1)
    causal_mask = jnp.tril(jnp.ones((BLK, BLK), dtype=bool))
    cum_t = jnp.moveaxis(cumulative, 1, -1)
    gaps = cum_t[..., :, None] - cum_t[..., None, :]
    decays = jnp.where(causal_mask, jnp.exp(jnp.where(causal_mask, gaps, 0.0)), 0.0)
    affinity = jnp.einsum("blgn,bsgn->bgls", c_rows, b_rows, precision=exact_mode)
    y_diag = jnp.einsum(
        "bghls,bsghp->blghp", affinity[:, :, None] * decays, scaled, precision=exact_mode
    )
    to_end = jnp.exp(cumulative[:, -1:] - cumulative)
    states = jnp.einsum(
        "blgn,blghp->bghpn", b_rows, scaled * to_end[..., None], precision=exact_mode
    )
    block_decay = jnp.exp(cumulative[:, -1])

    def advance(running, inputs):
        block_state, decay_now = inputs
        return (decay_now[..., None, None] * running + block_state, running)

    first_state = starting_state.reshape(groups, per_group, head_size, state_size)
    closing_state, incoming_state = lax.scan(advance, first_state, (states, block_decay))
    y_off = (
        jnp.einsum("blgn,bghpn->blghp", c_rows, incoming_state, precision=exact_mode)
        * jnp.exp(cumulative)[..., None]
    )
    result_rows = (y_diag + y_off).reshape(length, head_count, head_size)
    return (result_rows, closing_state.reshape(head_count, head_size, state_size))


def span_final_state(input_heads, time_step, decay_speed, sudden_decay, input_vector_groups):
    length, head_count, head_size = input_heads.shape
    groups = input_vector_groups.shape[1]
    log_decay_total = sudden_decay - time_step * decay_speed[None, :]
    sum_total = jnp.sum(log_decay_total, axis=0)
    after = sum_total[None, :] - jnp.cumsum(log_decay_total, axis=0)
    weighted = (input_heads * (time_step * jnp.exp(after))[:, :, None]).reshape(
        length, groups, head_count // groups, head_size
    )
    result = jnp.einsum("tgn,tghp->ghpn", input_vector_groups, weighted, precision=exact_mode)
    return (result.reshape(head_count, head_size, -1), jnp.exp(sum_total))


def carried_weight(scanned_gradient, readout_groups, time_step, decay_speed, sudden_decay):
    length, head_count, head_size = scanned_gradient.shape
    groups = readout_groups.shape[1]
    log_decay_total = sudden_decay - time_step * decay_speed[None, :]
    weighted = (
        scanned_gradient * jnp.exp(jnp.cumsum(log_decay_total, axis=0))[:, :, None]
    ).reshape(length, groups, head_count // groups, head_size)
    result = jnp.einsum("tgn,tghp->ghpn", readout_groups, weighted, precision=exact_mode)
    return result.reshape(head_count, head_size, -1)


def gate_norm(scan_out, gate_vals, group_norm_scale, groups):
    length = scan_out.shape[0]
    gated = scan_out.reshape(length, -1) * jax.nn.silu(gate_vals)
    grouped = gated.reshape(length, groups, -1)
    factor = lax.rsqrt(jnp.mean(grouped * grouped, axis=-1, keepdims=True) + norm_eps)
    return (grouped * factor).reshape(length, -1) * group_norm_scale[None, :]


def slot_choice(route_rows, expert_count, capacity):
    flat_routes = route_rows.reshape(-1)
    pairs = flat_routes.shape[0]
    onehot = flat_routes[:, None] == jnp.arange(expert_count, dtype=jnp.int32)[None, :]
    earlier = jnp.tril(jnp.ones((pairs, pairs), jnp.bfloat16), -1)
    before = jnp.dot(earlier, onehot.astype(jnp.bfloat16), preferred_element_type=jnp.float32)
    place = jnp.sum(jnp.where(onehot, before, 0.0), axis=1).astype(jnp.int32)
    destination = (flat_routes * capacity + place).reshape(route_rows.shape)
    slots = jnp.arange(expert_count * capacity, dtype=jnp.int32)
    return [slots[:, None] == destination[None, :, k] for k in range(route_rows.shape[1])]


def pack_rows(stream, grad_rows, chosen, weights):
    pick = sum(c.astype(jnp.bfloat16) for c in chosen)
    weight_of = sum(
        jnp.sum(jnp.where(c, weights[None, :, k], 0.0), axis=1) for k, c in enumerate(chosen)
    )
    routed = jnp.dot(pick, stream, preferred_element_type=jnp.float32).astype(jnp.bfloat16)
    picked = jnp.dot(pick, grad_rows, preferred_element_type=jnp.float32)
    return (routed, (picked * weight_of[:, None]).astype(jnp.bfloat16), pick)


def expert_hidden(routed_rows, routed_grads, w_gate, w_up, w_down):
    pre_gate = jnp.dot(routed_rows, w_gate, preferred_element_type=jnp.float32)
    pre_up = jnp.dot(routed_rows, w_up, preferred_element_type=jnp.float32)
    activated = jax.nn.silu(pre_gate)
    hidden = (activated * pre_up).astype(jnp.bfloat16)
    hidden_grad = lax.dot_general(
        routed_grads, w_down, (((1,), (1,)), ((), ())), preferred_element_type=jnp.float32
    )
    sigmoid_gate = jax.nn.sigmoid(pre_gate)
    gate_grad = (
        hidden_grad * pre_up * sigmoid_gate * (1.0 + pre_gate * (1.0 - sigmoid_gate))
    ).astype(jnp.bfloat16)
    up_grad = (hidden_grad * activated).astype(jnp.bfloat16)
    return (hidden, gate_grad, up_grad)


def expert_weight_grads(routed_rows, routed_grads, hidden, gate_grad, up_grad):
    contract = (((0,), (0,)), ((), ()))
    grad_g = lax.dot_general(routed_rows, gate_grad, contract, preferred_element_type=jnp.float32)
    grad_u = lax.dot_general(routed_rows, up_grad, contract, preferred_element_type=jnp.float32)
    grad_d = lax.dot_general(hidden, routed_grads, contract, preferred_element_type=jnp.float32)
    return (grad_g.astype(jnp.bfloat16), grad_u.astype(jnp.bfloat16), grad_d.astype(jnp.bfloat16))


def row_partial(gate_grad, up_grad, w_gate, w_up):
    contract = (((1,), (1,)), ((), ()))
    partial_sum = lax.dot_general(gate_grad, w_gate, contract, preferred_element_type=jnp.float32)
    partial_sum = partial_sum + lax.dot_general(
        up_grad, w_up, contract, preferred_element_type=jnp.float32
    )
    return lax.optimization_barrier(partial_sum.astype(jnp.bfloat16)).astype(jnp.float32)


def add_returns(grad_rows, returned, pick):
    gathered = lax.dot_general(
        pick, returned, (((0,), (0,)), ((), ())), preferred_element_type=jnp.float32
    )
    return (grad_rows.astype(jnp.float32) + gathered).astype(jnp.bfloat16)


def body(
    mixer_output_stream,
    layer_output_gradient,
    routes,
    expert_combine_weight,
    expert_gate_weight,
    expert_up_weight,
    expert_down_weight,
    head_mixer_input,
    head_step_size,
    head_decay_rate,
    extra_log_decay,
    state_entering_span,
    state_input_vectors,
    state_readout_vectors,
    gate_preactivation,
    group_norm_scale,
    mixer_output_weight,
):
    expert_count = lax.axis_size("sp")
    local_tokens = routes.shape[0]
    capacity = 3 * local_tokens // expert_count
    chosen = slot_choice(routes, expert_count, capacity)
    w_gate = expert_gate_weight[0]
    w_up = expert_up_weight[0]
    w_down = expert_down_weight[0]
    sent_rows, sent_grads, pick = pack_rows(
        mixer_output_stream, layer_output_gradient, chosen, expert_combine_weight
    )
    columns_here = sent_rows.shape[1]
    parts = lax.all_to_all(
        jnp.concatenate([sent_rows, sent_grads], axis=1).reshape(expert_count, capacity, -1),
        "sp",
        split_axis=0,
        concat_axis=0,
        tiled=True,
    )
    part_rows, part_grads = (parts[:, :, :columns_here], parts[:, :, columns_here:])
    whole_weight = lax.all_gather(mixer_output_weight, "sp", axis=1, tiled=True)
    routed_rows, routed_grads = (
        lax.all_gather(part_rows, "tp", axis=2, tiled=True),
        lax.all_gather(part_grads, "tp", axis=2, tiled=True),
    )
    head_local = head_step_size.shape[1]
    group_local = state_input_vectors.shape[1] // STATE
    input_heads = head_mixer_input.astype(jnp.float32).reshape(local_tokens, head_local, HDIM)
    input_vector_groups = state_input_vectors.astype(jnp.float32).reshape(
        local_tokens, group_local, STATE
    )
    readout_groups = state_readout_vectors.astype(jnp.float32).reshape(
        local_tokens, group_local, STATE
    )
    within_span_state, within_span_decay = span_final_state(
        input_heads, head_step_size, head_decay_rate, extra_log_decay, input_vector_groups
    )
    incoming_state, span_decays = state_before(
        within_span_state, within_span_decay, state_entering_span, "sp"
    )

    def forward(input_values, time_step_values, input_vector_entries, readout_entries):
        return span_local_scan(
            input_values,
            time_step_values,
            head_decay_rate,
            extra_log_decay,
            input_vector_entries,
            readout_entries,
            incoming_state,
        )

    (scan_out, closing_state), pull_back = jax.vjp(
        forward, input_heads, head_step_size, input_vector_groups, readout_groups
    )

    def apply_norm(scan_vals, gate_vals):
        return gate_norm(scan_vals, gate_vals, group_norm_scale, group_local)

    normed, pull_norm = jax.vjp(apply_norm, scan_out, gate_preactivation.astype(jnp.float32))
    normed_low = normed.astype(jnp.bfloat16)
    normed_all = lax.all_gather(normed_low, "sp", axis=0, tiled=True)
    routed_rows, normed_low = lax.optimization_barrier((routed_rows, normed_low))
    model_width = routed_rows.shape[2]
    routed_rows = routed_rows.reshape(-1, model_width)
    routed_grads = routed_grads.reshape(-1, model_width)
    hidden, gate_grad, up_grad = expert_hidden(routed_rows, routed_grads, w_gate, w_up, w_down)
    grad_g, grad_u, grad_d = expert_weight_grads(
        routed_rows, routed_grads, hidden, gate_grad, up_grad
    )
    partial_rows = row_partial(gate_grad, up_grad, w_gate, w_up)
    partial_rows = partial_rows.astype(jnp.bfloat16)
    arrived = (
        lax.all_to_all(
            partial_rows.reshape(partial_rows.shape[0], lax.axis_size("tp"), -1).swapaxes(0, 1),
            "tp",
            split_axis=0,
            concat_axis=0,
            tiled=True,
        )
    )
    summed = jnp.sum(arrived.astype(jnp.float32), axis=0).astype(jnp.bfloat16)
    returned = lax.all_to_all(
        summed.reshape(expert_count, capacity, -1), "sp", split_axis=0, concat_axis=0, tiled=True
    )
    returned, whole_weight = lax.optimization_barrier((returned, whole_weight))
    own_cols = add_returns(
        layer_output_gradient, returned.reshape(expert_count * capacity, -1), pick
    )
    mix_grad = lax.all_gather(own_cols, "tp", axis=1, tiled=True)
    mix_columns = lax.all_to_all(mix_grad, "sp", split_axis=1, concat_axis=0, tiled=True)
    proj_grad = lax.dot_general(
        normed_all, mix_columns, (((0,), (0,)), ((), ())), preferred_element_type=jnp.float32
    )
    columns = mix_grad
    normed_grad = lax.dot_general(
        columns,
        whole_weight,
        (((1,), (1,)), ((), ())),
        preferred_element_type=jnp.float32,
    )
    scanned_gradient, gate_grad_in = pull_norm(normed_grad)
    reached_gradient = carried_weight(
        scanned_gradient, readout_groups, head_step_size, head_decay_rate, extra_log_decay
    )
    later_grad = gradient_after(reached_gradient, span_decays, "sp")
    input_grad, step_grad, b_grad, c_grad = pull_back((scanned_gradient, later_grad))
    return (
        grad_g[None],
        grad_u[None],
        grad_d[None],
        proj_grad,
        input_grad.reshape(local_tokens, -1).astype(jnp.bfloat16),
        step_grad,
        b_grad.reshape(local_tokens, -1).astype(jnp.bfloat16),
        c_grad.reshape(local_tokens, -1).astype(jnp.bfloat16),
        gate_grad_in.astype(jnp.bfloat16),
    )


def solution(mesh):
    return jax.shard_map(
        body,
        mesh=mesh,
        in_specs=(
            P("sp", "tp"),
            P("sp", "tp"),
            P("sp", None),
            P("sp", None),
            P("sp", None, "tp"),
            P("sp", None, "tp"),
            P("sp", "tp", None),
            P("sp", "tp"),
            P("sp", "tp"),
            P("tp"),
            P("sp", "tp"),
            P("tp", None, None),
            P("sp", "tp"),
            P("sp", "tp"),
            P("sp", "tp"),
            P("tp"),
            P("tp", "sp"),
        ),
        out_specs=(
            P("sp", None, "tp"),
            P("sp", None, "tp"),
            P("sp", "tp", None),
            P("tp", "sp"),
            P("sp", "tp"),
            P("sp", "tp"),
            P("sp", "tp"),
            P("sp", "tp"),
            P("sp", "tp"),
        ),
        check_vma=False,
    )
```

profile of v0, /device:TPU:0, one launch (start us, length us, event | category | flops | bytes accessed | tf_op | source)
XLA Modules:
  0.0 249.0 jit_solution(14573435765564554305)
XLA Ops:
  11.9 27.3 %all_to_all.54 = bf16[8,48,1024]{2,1,0:T(8,128)(2,1)S(1)} all-to-all(bf16[8,48,1024]{2,1,0:T(8,128)(2,1)S(1)} %bitcast.305), channel_id=1, replica_groups=mesh['sp'=8,'tp'=4] {'sp'}, dimensions={0} | all-to-all | bytes 1572864 | tf_op jit(solution)/shard_map/all_to_all | solution.py:227
  43.8 3.6 %all-to-all-start.1 = ((bf16[8,129,128]{2,1,0:T(8,128)(2,1)}), bf16[8,129,128]{2,1,0:T(8,128)(2,1)S(1)}, u32[]{:S(2)}, u32[]{:S(2)}) async-start(bf16[8,129,128]{2,1,0:T(8,128)(2,1)} %pad_maximum_fusion.1), calls=%async_computation.1 | async-start | bytes 557056 | tf_op jit(solution)/shard_map/all_to_all | solution.py:16
  48.4 1.5 constant_dynamic-update-slice_fusion.7
  50.0 6.3 %all-to-all-done.1 = bf16[8,129,128]{2,1,0:T(8,128)(2,1)S(1)} async-done(((bf16[8,129,128]{2,1,0:T(8,128)(2,1)}), bf16[8,129,128]{2,1,0:T(8,128)(2,1)S(1)}, u32[]{:S(2)}, u32[]{:S(2)}) %all-to-all-start.1) | async-done | bytes 264224 | tf_op jit(solution)/shard_map/all_to_all | solution.py:16
  56.9 1.6 constant_dynamic-update-slice_fusion.6
  62.8 3.7 %all-to-all-start.2 = ((bf16[8,128,128]{2,1,0:T(8,128)(2,1)}), bf16[8,128,128]{2,1,0:T(8,128)(2,1)S(1)}, u32[]{:S(2)}, u32[]{:S(2)}) async-start(bf16[8,128,128]{2,1,0:T(8,128)(2,1)} %constant_dynamic-update-slice_fusion), calls=%async_computation.2 | async-start | bytes 524288 | tf_op jit(solution)/shard_map/all_to_all | solution.py:16
  67.2 7.8 %all-to-all-done.2 = bf16[8,128,128]{2,1,0:T(8,128)(2,1)S(1)} async-done(((bf16[8,128,128]{2,1,0:T(8,128)(2,1)}), bf16[8,128,128]{2,1,0:T(8,128)(2,1)S(1)}, u32[]{:S(2)}, u32[]{:S(2)}) %all-to-all-start.2) | async-done | bytes 262176 | tf_op jit(solution)/shard_map/all_to_all | solution.py:16
  79.0 4.5 %fusion.2 = f32[384,896]{1,0:T(8,128)S(1)} fusion(bf16[384,2048]{1,0:T(8,128)(2,1)} %bitcast.334, bf16[1,2048,896]{2,1,0:T(8,128)(2,1)} %param.21), kind=kOutput, calls=%fused_computation.2 | convolution fusion | flops 1409286144 | bytes 6619136 | tf_op jit(solution)/shard_map/dot_general | solution.py:158
  83.5 2.9 %fusion.6 = f32[384,896]{1,0:T(8,128)} fusion(bf16[384,2048]{1,0:T(8,128)(2,1)S(1)} %bitcast.337, bf16[1,2048,896]{2,1,0:T(8,128)(2,1)S(1)} %copy-done.57), kind=kOutput, calls=%fused_computation.6 | convolution fusion | flops 1409286144 | bytes 6619136 | tf_op jit(solution)/shard_map/dot_general | solution.py:159
  86.4 5.1 %multiply_convert_fusion.1 = (bf16[384,896]{1,0:T(8,128)(2,1)S(1)}, bf16[384,896]{1,0:T(8,128)(2,1)S(1)}) fusion(f32[384,896]{1,0:T(8,128)S(1)} %fusion.2, f32[384,896]{1,0:T(8,128)} %fusion.6, bf16[384,2048]{1,0:T(8,128)(2,1)} %bitcast.338, bf16[1,896,2048]{2,1,0:T(8,128)(2,1)} %param.23), kind=kOutput, calls=%fused_computation.16 | convolution fusion | flops 1413758976 | bytes 9371648 | tf_op jit(solution)/shard_map/dot_general | solution.py:162
  91.5 1.8 fusion
  94.1 1.8 add_convert_fusion
  95.9 1.3 copy.378
  97.2 3.7 %all-to-all-start.3 = ((bf16[4,384,512]{2,1,0:T(8,128)(2,1)}), bf16[4,384,512]{2,1,0:T(8,128)(2,1)S(1)}, u32[]{:S(2)}, u32[]{:S(2)}) async-start(bf16[4,384,512]{2,1,0:T(8,128)(2,1)} %bitcast.298), calls=%async_computation.3 | async-start | bytes 3145728 | tf_op jit(solution)/shard_map/all_to_all | solution.py:288
  101.6 19.3 %all-to-all-done.3 = bf16[4,384,512]{2,1,0:T(8,128)(2,1)S(1)} async-done(((bf16[4,384,512]{2,1,0:T(8,128)(2,1)}), bf16[4,384,512]{2,1,0:T(8,128)(2,1)S(1)}, u32[]{:S(2)}, u32[]{:S(2)}) %all-to-all-start.3) | async-done | bytes 1572896 | tf_op jit(solution)/shard_map/all_to_all | solution.py:288
  122.0 3.8 %all-to-all-start.4 = ((bf16[8,48,512]{2,1,0:T(8,128)(2,1)}), bf16[8,48,512]{2,1,0:T(8,128)(2,1)S(1)}, u32[]{:S(2)}, u32[]{:S(2)}) async-start(bf16[8,48,512]{2,1,0:T(8,128)(2,1)} %bitcast.312), calls=%async_computation.4 | async-start | bytes 786432 | tf_op jit(solution)/shard_map/all_to_all | solution.py:297
  125.8 5.8 %convert_bitcast_fusion.1 = bf16[1,2048,896]{2,1,0:T(8,128)(2,1)} fusion(bf16[384,2048]{1,0:T(8,128)(2,1)} %bitcast.335, bf16[384,896]{1,0:T(8,128)(2,1)} %copy-done.65), kind=kOutput, calls=%fused_computation.11 | convolution fusion | flops 1411121152 | bytes 5931008 | tf_op jit(solution)/shard_map/dot_general | solution.py:176
  131.7 4.0 %convert_bitcast_fusion = bf16[1,896,2048]{2,1,0:T(8,128)(2,1)} fusion(bf16[384,2048]{1,0:T(8,128)(2,1)S(1)} %bitcast.339, f32[384,896]{1,0:T(8,128)S(1)} %copy-done.64, f32[384,896]{1,0:T(8,128)S(1)} %copy-done.63), kind=kOutput, calls=%fused_computation.10 | convolution fusion | flops 1413185536 | bytes 7995392 | tf_op jit(solution)/shard_map/dot_general | solution.py:177
  135.7 12.2 %all-to-all-done.4 = bf16[8,48,512]{2,1,0:T(8,128)(2,1)S(1)} async-done(((bf16[8,48,512]{2,1,0:T(8,128)(2,1)}), bf16[8,48,512]{2,1,0:T(8,128)(2,1)S(1)}, u32[]{:S(2)}, u32[]{:S(2)}) %all-to-all-start.4) | async-done | bytes 393248 | tf_op jit(solution)/shard_map/all_to_all | solution.py:297
  147.9 16.7 %all-gather.11.cloned.1.call-done = bf16[1024,2048]{1,0:T(8,128)(2,1)} async-done(((bf16[1024,256]{1,0:T(8,128)(2,1)}), bf16[1024,2048]{1,0:T(8,128)(2,1)}) %all-gather.11.cloned.1.call-update) | async-done | bytes 4194320 | tf_op jit(solution)/shard_map/all_gather | solution.py:235
  165.0 8.3 %all_gather.19 = bf16[128,2048]{1,0:T(8,128)(2,1)S(1)} all-gather(bf16[128,512]{1,0:T(8,128)(2,1)S(1)} %fusion.16), channel_id=1, replica_groups=mesh['sp'=8,'tp'=4] {'tp'}, dimensions={1}, use_global_device_ids=true | all-gather | bytes 655360 | tf_op jit(solution)/shard_map/all_gather | solution.py:304
  173.2 4.9 %fusion.111 = (f32[128,1024]{1,0:T(8,128)}, f32[128,1024]{1,0:T(8,128)}) fusion(f32[128,1024]{1,0:T(8,128)S(1)} %copy.322, bf16[128,1024]{1,0:T(8,128)(2,1)S(1)} %copy-done.5, f32[1024]{0:T(1024)S(1)} %copy-done.53, bf16[128,2048]{1,0:T(8,128)(2,1)S(1)} %all_gather.19, bf16[1024,2048]{1,0:T(8,128)(2,1)} %all-gather.11.cloned.1.call-done), kind=kOutput, calls=%fused_computation.209 | convolution fusion | flops 537919488 | bytes 6557696 | tf_op jit(solution)/shard_map/dot_general | solution.py:310
  178.1 1.5 mul.564
  183.4 3.7 %all-to-all-start.6 = ((bf16[8,128,128]{2,1,0:T(8,128)(2,1)}), bf16[8,128,128]{2,1,0:T(8,128)(2,1)S(1)}, u32[]{:S(2)}, u32[]{:S(2)}) async-start(bf16[8,128,128]{2,1,0:T(8,128)(2,1)} %bitcast.62), calls=%async_computation.6 | async-start | bytes 524288 | tf_op jit(solution)/shard_map/all_to_all | solution.py:16
  187.1 5.7 %convert_bitcast_fusion.2 = bf16[1,2048,896]{2,1,0:T(8,128)(2,1)} fusion(bf16[384,2048]{1,0:T(8,128)(2,1)} %bitcast.336, bf16[384,896]{1,0:T(8,128)(2,1)} %copy-done.61), kind=kOutput, calls=%fused_computation.12 | convolution fusion | flops 1411121152 | bytes 5931008 | tf_op jit(solution)/shard_map/dot_general | solution.py:175
  193.3 1.6 fusion.26
  194.9 3.1 %all-to-all-done.6 = bf16[8,128,128]{2,1,0:T(8,128)(2,1)S(1)} async-done(((bf16[8,128,128]{2,1,0:T(8,128)(2,1)}), bf16[8,128,128]{2,1,0:T(8,128)(2,1)S(1)}, u32[]{:S(2)}, u32[]{:S(2)}) %all-to-all-start.6) | async-done | bytes 262176 | tf_op jit(solution)/shard_map/all_to_all | solution.py:16
  203.5 4.0 %all-to-all-start.7 = ((bf16[8,128,128]{2,1,0:T(8,128)(2,1)}), bf16[8,128,128]{2,1,0:T(8,128)(2,1)S(1)}, u32[]{:S(2)}, u32[]{:S(2)}) async-start(bf16[8,128,128]{2,1,0:T(8,128)(2,1)} %constant_dynamic-update-slice_fusion.8), calls=%async_computation.7 | async-start | bytes 524288 | tf_op jit(solution)/shard_map/all_to_all | solution.py:16
  209.5 11.2 %all-to-all-done.7 = bf16[8,128,128]{2,1,0:T(8,128)(2,1)S(1)} async-done(((bf16[8,128,128]{2,1,0:T(8,128)(2,1)}), bf16[8,128,128]{2,1,0:T(8,128)(2,1)S(1)}, u32[]{:S(2)}, u32[]{:S(2)}) %all-to-all-start.7) | async-done | bytes 262176 | tf_op jit(solution)/shard_map/all_to_all | solution.py:16
  220.8 3.5 %all-to-all-start.5 = ((bf16[128,8,256]{2,0,1:T(8,128)(2,1)}), bf16[128,8,256]{2,0,1:T(8,128)(2,1)S(1)}, u32[]{:S(2)}, u32[]{:S(2)}) async-start(bf16[128,8,256]{2,0,1:T(8,128)(2,1)} %bitcast.287), calls=%async_computation.5 | async-start | bytes 1048576 | tf_op jit(solution)/shard_map/all_to_all | solution.py:305
  230.4 8.7 %all-to-all-done.5 = bf16[128,8,256]{2,0,1:T(8,128)(2,1)S(1)} async-done(((bf16[128,8,256]{2,0,1:T(8,128)(2,1)}), bf16[128,8,256]{2,0,1:T(8,128)(2,1)S(1)}, u32[]{:S(2)}, u32[]{:S(2)}) %all-to-all-start.5) | async-done | bytes 524320 | tf_op jit(solution)/shard_map/all_to_all | solution.py:305
  239.1 3.3 %fusion.122 = f32[1024,256]{1,0:T(8,128)} fusion(bf16[1024,1024]{1,0:T(8,128)(2,1)} %all-gather.9.cloned.1.call-done, bf16[1024,256]{1,0:T(8,128)(2,1)S(1)} %bitcast.319), kind=kOutput, calls=%fused_computation.216 | convolution fusion | flops 536870912 | bytes 3670016 | tf_op jit(solution)/shard_map/dot_general | solution.py:306
  (254 shorter events, 40.2 us)
Async XLA Ops:
  7.2 71.8 %all-gather.5.cloned.1.call-start = ((), (), s32[]{:S(2)}) async-start(), calls=%async_computation.8 | async-start | bytes 1966080 | tf_op jit(solution)/shard_map/all_gather | solution.py:237
  40.2 46.2 %all-gather.7.cloned.1.call-start = ((), (), s32[]{:S(2)}) async-start(), calls=%async_computation.9 | async-start | bytes 1966080 | tf_op jit(solution)/shard_map/all_gather | solution.py:238
  42.5 23.9 %copy-start.8 = (bf16[128,2,128]{2,1,0:T(2,128)(2,1)}, bf16[128,2,128]{2,1,0:T(2,128)(2,1)S(1)}, u32[]{:S(2)}) copy-start(bf16[128,2,128]{2,1,0:T(2,128)(2,1)S(1)} %reshape.598) | copy-start | bytes 196612
  43.8 12.5 %all-to-all-start.1 = ((bf16[8,129,128]{2,1,0:T(8,128)(2,1)}), bf16[8,129,128]{2,1,0:T(8,128)(2,1)S(1)}, u32[]{:S(2)}, u32[]{:S(2)}) async-start(bf16[8,129,128]{2,1,0:T(8,128)(2,1)} %pad_maximum_fusion.1), calls=%async_computation.1 | async-start | bytes 557056 | tf_op jit(solution)/shard_map/all_to_all | solution.py:16
  47.4 117.2 %all-gather.11.cloned.1.call-start = ((), (), s32[]{:S(2)}) async-start(), calls=%async_computation.11 | async-start | bytes 4718592 | tf_op jit(solution)/shard_map/all_gather | solution.py:235
  50.0 16.6 %copy-start.24 = (bf16[128,256]{1,0:T(8,128)(2,1)S(1)}, bf16[128,256]{1,0:T(8,128)(2,1)}, u32[]{:S(2)}) copy-start(bf16[128,256]{1,0:T(8,128)(2,1)} %param.30) | copy-start | bytes 196612
  62.8 12.2 %all-to-all-start.2 = ((bf16[8,128,128]{2,1,0:T(8,128)(2,1)}), bf16[8,128,128]{2,1,0:T(8,128)(2,1)S(1)}, u32[]{:S(2)}, u32[]{:S(2)}) async-start(bf16[8,128,128]{2,1,0:T(8,128)(2,1)} %constant_dynamic-update-slice_fusion), calls=%async_computation.2 | async-start | bytes 524288 | tf_op jit(solution)/shard_map/all_to_all | solution.py:16
  66.4 10.0 %copy-start.28 = (pred[128,128]{1,0:T(8,128)(4,1)}, pred[128,128]{1,0:T(8,128)(4,1)S(1)}, u32[]{:S(2)}) copy-start(pred[128,128]{1,0:T(8,128)(4,1)S(1)} %iota_compare_fusion.3) | copy-start | bytes 49156
  66.6 8.4 %copy-start.14 = (bf16[128,2,128]{0,2,1:T(8,128)(2,1)}, bf16[128,2,128]{0,2,1:T(8,128)(2,1)S(1)}, u32[]{:S(2)}) copy-start(bf16[128,2,128]{0,2,1:T(8,128)(2,1)S(1)} %copy.342) | copy-start | bytes 196612
  66.6 9.8 %copy-start.10 = (bf16[128,2,128]{2,1,0:T(2,128)(2,1)}, bf16[128,2,128]{2,1,0:T(2,128)(2,1)S(1)}, u32[]{:S(2)}) copy-start(bf16[128,2,128]{2,1,0:T(2,128)(2,1)S(1)} %reshape.597) | copy-start | bytes 196612
  66.8 8.1 %copy-start.12 = (bf16[128,2,128]{0,2,1:T(8,128)(2,1)}, bf16[128,2,128]{0,2,1:T(8,128)(2,1)S(1)}, u32[]{:S(2)}) copy-start(bf16[128,2,128]{0,2,1:T(8,128)(2,1)S(1)} %copy.341) | copy-start | bytes 196612
  66.9 9.5 %copy-start.41 = (f32[2,8,128]{2,1,0:T(8,128)}, f32[2,8,128]{2,1,0:T(8,128)S(1)}, u32[]{:S(2)}) copy-start(f32[2,8,128]{2,1,0:T(8,128)S(1)} %copy.314) | copy-start | bytes 24580
  66.9 9.5 %copy-start.26 = (f32[128,2,8]{0,2,1:T(8,128)}, f32[128,2,8]{0,2,1:T(8,128)S(1)}, u32[]{:S(2)}) copy-start(f32[128,2,8]{0,2,1:T(8,128)S(1)} %bitcast_exponential_fusion) | copy-start | bytes 24580
  67.2 9.3 %copy-start.21 = (f32[2,128,128]{2,1,0:T(8,128)}, f32[2,128,128]{2,1,0:T(8,128)S(1)}, u32[]{:S(2)}) copy-start(f32[2,128,128]{2,1,0:T(8,128)S(1)} %fusion.121) | copy-start | bytes 393220
  97.2 23.7 %all-to-all-start.3 = ((bf16[4,384,512]{2,1,0:T(8,128)(2,1)}), bf16[4,384,512]{2,1,0:T(8,128)(2,1)S(1)}, u32[]{:S(2)}, u32[]{:S(2)}) async-start(bf16[4,384,512]{2,1,0:T(8,128)(2,1)} %bitcast.298), calls=%async_computation.3 | async-start | bytes 3145728 | tf_op jit(solution)/shard_map/all_to_all | solution.py:288
  100.9 129.5 %all-gather.9.cloned.1.call-start = ((), (), s32[]{:S(2)}) async-start(), calls=%async_computation.10 | async-start | bytes 2359296 | tf_op jit(solution)/shard_map/all_gather | solution.py:276
  122.0 25.9 %all-to-all-start.4 = ((bf16[8,48,512]{2,1,0:T(8,128)(2,1)}), bf16[8,48,512]{2,1,0:T(8,128)(2,1)S(1)}, u32[]{:S(2)}, u32[]{:S(2)}) async-start(bf16[8,48,512]{2,1,0:T(8,128)(2,1)} %bitcast.312), calls=%async_computation.4 | async-start | bytes 786432 | tf_op jit(solution)/shard_map/all_to_all | solution.py:297
  131.6 33.0 %copy-start.16 = (bf16[128,512]{1,0:T(8,128)(2,1)S(1)}, bf16[128,512]{1,0:T(8,128)(2,1)}, u32[]{:S(2)}) copy-start(bf16[128,512]{1,0:T(8,128)(2,1)} %param.18) | copy-start | bytes 393220
  131.7 33.0 %copy-start.35 = (s32[128]{0:T(128)S(1)}, s32[128]{0:T(128)}, u32[]{:S(2)}) copy-start(s32[128]{0:T(128)} %copy-done.34) | copy-start | bytes 1540
  131.7 33.0 %copy-start.37 = (s32[128]{0:T(128)S(1)}, s32[128]{0:T(128)}, u32[]{:S(2)}) copy-start(s32[128]{0:T(128)} %copy-done.36) | copy-start | bytes 1540
  131.7 41.5 %copy-start.5 = (bf16[128,1024]{1,0:T(8,128)(2,1)S(1)}, bf16[128,1024]{1,0:T(8,128)(2,1)}, u32[]{:S(2)}) copy-start(bf16[128,1024]{1,0:T(8,128)(2,1)} %param.31) | copy-start | bytes 786436
  131.7 41.5 %copy-start.53 = (f32[1024]{0:T(1024)S(1)}, f32[1024]{0:T(1024)}, u32[]{:S(2)}) copy-start(f32[1024]{0:T(1024)} %param.32) | copy-start | bytes 12292
  183.4 14.6 %all-to-all-start.6 = ((bf16[8,128,128]{2,1,0:T(8,128)(2,1)}), bf16[8,128,128]{2,1,0:T(8,128)(2,1)S(1)}, u32[]{:S(2)}, u32[]{:S(2)}) async-start(bf16[8,128,128]{2,1,0:T(8,128)(2,1)} %bitcast.62), calls=%async_computation.6 | async-start | bytes 524288 | tf_op jit(solution)/shard_map/all_to_all | solution.py:16
  187.1 6.1 %copy-start.22 = (f32[2,128,128]{2,1,0:T(8,128)S(1)}, f32[2,128,128]{2,1,0:T(8,128)}, u32[]{:S(2)}) copy-start(f32[2,128,128]{2,1,0:T(8,128)} %copy-done.21) | copy-start | bytes 393220
  187.1 6.1 %copy-start.29 = (pred[128,128]{1,0:T(8,128)(4,1)S(1)}, pred[128,128]{1,0:T(8,128)(4,1)}, u32[]{:S(2)}) copy-start(pred[128,128]{1,0:T(8,128)(4,1)} %copy-done.28) | copy-start | bytes 49156
  187.1 6.1 %copy-start.42 = (f32[2,8,128]{2,1,0:T(8,128)S(1)}, f32[2,8,128]{2,1,0:T(8,128)}, u32[]{:S(2)}) copy-start(f32[2,8,128]{2,1,0:T(8,128)} %copy-done.41) | copy-start | bytes 24580
  194.9 12.6 %copy-start.15 = (bf16[128,2,128]{0,2,1:T(8,128)(2,1)S(1)}, bf16[128,2,128]{0,2,1:T(8,128)(2,1)}, u32[]{:S(2)}) copy-start(bf16[128,2,128]{0,2,1:T(8,128)(2,1)} %copy-done.14) | copy-start | bytes 196612
  198.9 10.4 %copy-start.13 = (bf16[128,2,128]{0,2,1:T(8,128)(2,1)S(1)}, bf16[128,2,128]{0,2,1:T(8,128)(2,1)}, u32[]{:S(2)}) copy-start(bf16[128,2,128]{0,2,1:T(8,128)(2,1)} %copy-done.12) | copy-start | bytes 196612
  198.9 10.5 %copy-start.7 = (f32[1,128,2,8,64]{1,4,3,2,0:T(8,128)S(1)}, f32[1,128,2,8,64]{1,4,3,2,0:T(8,128)}, u32[]{:S(2)}) copy-start(f32[1,128,2,8,64]{1,4,3,2,0:T(8,128)} %copy-done.6) | copy-start | bytes 1572868
  203.5 17.3 %all-to-all-start.7 = ((bf16[8,128,128]{2,1,0:T(8,128)(2,1)}), bf16[8,128,128]{2,1,0:T(8,128)(2,1)S(1)}, u32[]{:S(2)}, u32[]{:S(2)}) async-start(bf16[8,128,128]{2,1,0:T(8,128)(2,1)} %constant_dynamic-update-slice_fusion.8), calls=%async_computation.7 | async-start | bytes 524288 | tf_op jit(solution)/shard_map/all_to_all | solution.py:16
  209.3 15.5 %copy-start.9 = (bf16[128,2,128]{2,1,0:T(2,128)(2,1)S(1)}, bf16[128,2,128]{2,1,0:T(2,128)(2,1)}, u32[]{:S(2)}) copy-start(bf16[128,2,128]{2,1,0:T(2,128)(2,1)} %copy-done.8) | copy-start | bytes 196612
  220.8 18.3 %all-to-all-start.5 = ((bf16[128,8,256]{2,0,1:T(8,128)(2,1)}), bf16[128,8,256]{2,0,1:T(8,128)(2,1)S(1)}, u32[]{:S(2)}, u32[]{:S(2)}) async-start(bf16[128,8,256]{2,0,1:T(8,128)(2,1)} %bitcast.287), calls=%async_computation.5 | async-start | bytes 1048576 | tf_op jit(solution)/shard_map/all_to_all | solution.py:305
  (45 other events, 155.1 us)
Sparse Core Ops, SparseCore 0:
  40.3 18.6 all-gather.4
  61.1 19.6 all-gather.6
  82.8 81.8 all-gather.10
  166.7 54.3 all-gather.8
where the time goes:
time: 250 us; the launch traced here: 249 us
  waiting for transfers between devices  86.8 us (35%)
  matrix products  48.4 us (19%)
  blocking collectives  35.5 us (14%)
  starting transfers between devices  26 us (10%)
  other arithmetic  19.1 us (8%)
  local copies, waits for them, and re-layouts  18.2 us (7%)
  between operations  14.8 us (6%)
    all_to_all x4, waiting for transfers between devices, span_rows(): lax.all_to_all(x.astype(jnp.bfloat16), axis, split_axis=0, concat_axis=0,...  28.5 us
    all_to_all x1, blocking collectives, body(): lax.all_to_all(jnp.concatenate([sent_rows, sent_grads], axis=1).reshape(e...  27.3 us
    all_to_all x1, waiting for transfers between devices, body(): lax.all_to_all(partial_rows.reshape(partial_rows.shape[0], lax.axis_size(...  19.3 us
    all_gather x1, waiting for transfers between devices, body(): whole_weight = lax.all_gather(mixer_output_weight, 'sp', axis=1, tiled=True)  16.7 us
    all_to_all x4, starting transfers between devices, span_rows(): lax.all_to_all(x.astype(jnp.bfloat16), axis, split_axis=0, concat_axis=0,...  14.9 us
    all_to_all x1, waiting for transfers between devices, body(): lax.all_to_all(summed.reshape(expert_count, capacity, -1), 'sp', split_ax...  12.2 us
    unnamed x12, other arithmetic  9.24 us
    all_to_all x1, waiting for transfers between devices, body(): lax.all_to_all(mix_grad, 'sp', split_axis=1, concat_axis=0, tiled=True)  8.7 us
  transfers between devices with their start and end apart: 11, of which 8 were waited for; matrix products, arithmetic and copies ran while one was open for 30% of the time, Pallas kernels for 0%

commit v1 on v0

--- a/solution.py
+++ b/solution.py
@@ -1,6 +1,10 @@
+import functools
+
 import jax
 import jax.numpy as jnp
 from jax import lax
+from jax.experimental import pallas as pl
+from jax.experimental.pallas import tpu as pltpu
 from jax.sharding import PartitionSpec as P
 
 HDIM = 64
@@ -12,43 +16,509 @@
 exact_mode = lax.Precision.HIGH
 
 
-def span_rows(x, axis):
-    return lax.all_to_all(
-        x.astype(jnp.bfloat16), axis, split_axis=0, concat_axis=0, tiled=True
-    ).astype(jnp.float32)
-
-
-def state_before(state, decay, first_state, axis):
-    count, here = (lax.axis_size(axis), lax.axis_index(axis))
+MESH = pl.DeviceIdType.MESH
+BF16 = jnp.bfloat16
+F32 = jnp.float32
+DMA = pltpu.SemaphoreType.DMA
+
+
+class Place:
+    def __init__(self, n_sp, n_tp):
+        self.n_sp, self.n_tp = n_sp, n_tp
+        self.inner = 2 if n_tp % 2 == 0 else 1
+        self.outer = n_tp // self.inner
+        self.me = lax.axis_index("sp")
+        self.t = lax.axis_index("tp")
+        self.core = lax.rem(self.t, self.inner)
+        self.far = lax.div(self.t, self.inner)
+
+    def span(self, d):
+        return lax.rem(self.me + d, self.n_sp)
+
+    def span_back(self, d):
+        return lax.rem(self.me + (self.n_sp - d), self.n_sp)
+
+    def partners(self):
+        return [self.far * self.inner + lax.rem(self.core + i, self.inner) for i in range(1, self.inner)]
+
+    def outers(self):
+        return [lax.rem(self.far + j, self.outer) * self.inner + self.core for j in range(1, self.outer)]
+
+    def enter(self, with_span=True):
+        barrier = pltpu.get_barrier_semaphore()
+        devices = [(self.me, p) for p in self.partners() + self.outers()]
+        if with_span:
+            devices += [(self.span(d), self.t) for d in range(1, self.n_sp)]
+        for device in devices:
+            pl.semaphore_signal(barrier, inc=1, device_id=device, device_id_type=MESH)
+        pl.semaphore_wait(barrier, len(devices))
+
+
+def remote(src, dst, send, recv, device):
+    return pltpu.make_async_remote_copy(
+        src_ref=src, dst_ref=dst, send_sem=send, recv_sem=recv, device_id=device, device_id_type=MESH
+    )
+
+
+def decay_column(row, per):
+    width = row.shape[-1]
+    down = lax.broadcasted_iota(jnp.int32, (per, width), 0)
+    across = lax.broadcasted_iota(jnp.int32, (per, width), 1)
+    spread = jnp.broadcast_to(row.astype(F32), (per, width))
+    return jnp.sum(jnp.where(down == across, spread, 0.0), axis=1, keepdims=True)
+
+
+def dispatch_kernel(
+    n_sp,
+    n_tp,
+    rows_ref,
+    grads_ref,
+    state_ref,
+    first_ref,
+    rows_out,
+    grads_out,
+    before_out,
+    decays_out,
+    state_in,
+    before_tmp,
+    span_send,
+    tp_send,
+    fwd_send,
+    block_recv,
+    state_send,
+    state_recv,
+    back_send,
+    back_recv,
+):
+    at = Place(n_sp, n_tp)
+    me, t = at.me, at.t
+    width = rows_ref.shape[2]
+    per = first_ref.shape[0]
+
+    def cols(owner):
+        return pl.ds(pl.multiple_of(owner * width, width), width)
+
+    pairs = ((rows_ref, rows_out), (grads_ref, grads_out))
+    at.enter()
+    waits = []
+    for d in range(1, n_sp):
+        peer = at.span(d)
+        for a, (src, dst) in enumerate(pairs):
+            copy = remote(
+                src.at[peer],
+                dst.at[me, :, cols(t)],
+                span_send.at[a, d],
+                block_recv.at[a, me, t],
+                (peer, t),
+            )
+            copy.start()
+            waits.append(copy.wait_send)
+    for d in range(1, n_sp):
+        peer = at.span(d)
+        copy = remote(
+            state_ref.at[peer], state_in.at[me], state_send.at[d], state_recv.at[me], (peer, t)
+        )
+        copy.start()
+        waits.append(copy.wait_send)
+
+    def pass_on(d, sources, peers, owner, sems, base):
+        src_span = at.span_back(d)
+        for a in range(2):
+            for i, peer in enumerate(peers):
+                copy = remote(
+                    sources[a],
+                    pairs[a][1].at[src_span, :, cols(owner)],
+                    sems.at[a, d, base + i],
+                    block_recv.at[a, src_span, owner],
+                    (me, peer),
+                )
+                copy.start()
+                waits.append(copy.wait_send)
+
+    def landed(a, src_span, owner):
+        block = pairs[a][1].at[src_span, :, cols(owner)]
+        pltpu.make_async_copy(block, block, block_recv.at[a, src_span, owner]).wait()
+
+    near = at.outers() + at.partners()
+    pass_on(0, [rows_ref.at[me], grads_ref.at[me]], near, t, tp_send, 0)
+    rows_out[me, :, cols(t)] = rows_ref[me]
+    grads_out[me, :, cols(t)] = grads_ref[me]
+    state_in[me] = state_ref[me]
+    for d in range(1, n_sp):
+        src_span = at.span_back(d)
+        for a in range(2):
+            landed(a, src_span, t)
+        pass_on(d, [p[1].at[src_span, :, cols(t)] for p in pairs], near, t, tp_send, 0)
+
+    for d in range(1, n_sp):
+        src_span = at.span_back(d)
+        block = state_in.at[src_span]
+        pltpu.make_async_copy(block, block, state_recv.at[src_span]).wait()
+    running = first_ref[...]
+    for k in range(n_sp):
+        before_tmp[k] = running.astype(BF16)
+        line = state_in[k, per : per + 1]
+        decays_out[k] = line
+        running = decay_column(line, per) * running + state_in[k, :per].astype(F32)
+    for d in range(1, n_sp):
+        peer = at.span(d)
+        copy = remote(
+            before_tmp.at[peer], before_out.at[me], back_send.at[d], back_recv.at[me], (peer, t)
+        )
+        copy.start()
+        waits.append(copy.wait_send)
+    before_out[me] = before_tmp[me]
+
+    for d in range(n_sp):
+        src_span = at.span_back(d)
+        for j, owner in enumerate(at.outers()):
+            for a in range(2):
+                landed(a, src_span, owner)
+            pass_on(
+                d,
+                [p[1].at[src_span, :, cols(owner)] for p in pairs],
+                at.partners(),
+                owner,
+                fwd_send,
+                j * (at.inner - 1),
+            )
+    for d in range(n_sp):
+        src_span = at.span_back(d)
+        for partner in at.partners():
+            core = lax.rem(partner, at.inner)
+            for far in range(at.outer):
+                for a in range(2):
+                    landed(a, src_span, far * at.inner + core)
+    for d in range(1, n_sp):
+        src_span = at.span_back(d)
+        block = before_out.at[src_span]
+        pltpu.make_async_copy(block, block, back_recv.at[src_span]).wait()
+    for wait in waits:
+        wait()
+
+
+def whole(count):
+    return [pl.BlockSpec(memory_space=pltpu.VMEM)] * count
+
+
+def dispatch(rows, grads, state, first, n_tp):
+    n_sp, capacity, width = rows.shape
+    per, lanes = first.shape
+    inner = 2 if n_tp % 2 == 0 else 1
+    near = n_tp // inner - 1 + inner - 1
+    out = jax.ShapeDtypeStruct((n_sp, capacity, width * n_tp), BF16)
+    return pl.pallas_call(
+        functools.partial(dispatch_kernel, n_sp, n_tp),
+        out_shape=(
+            out,
+            out,
+            jax.ShapeDtypeStruct((n_sp, per, lanes), BF16),
+            jax.ShapeDtypeStruct((n_sp, 1, lanes), BF16),
+        ),
+        in_specs=whole(4),
+        out_specs=tuple(whole(4)),
+        scratch_shapes=[
+            pltpu.VMEM(state.shape, BF16),
+            pltpu.VMEM((n_sp, per, lanes), BF16),
+            DMA((2, n_sp)),
+            DMA((2, n_sp, max(near, 1))),
+            DMA((2, n_sp, max((n_tp // inner - 1) * (inner - 1), 1))),
+            DMA((2, n_sp, n_tp)),
+            DMA((n_sp,)),
+            DMA((n_sp,)),
+            DMA((n_sp,)),
+            DMA((n_sp,)),
+        ],
+        compiler_params=pltpu.CompilerParams(collective_id=1, has_side_effects=True),
+        cost_estimate=pl.CostEstimate(
+            flops=20_000_000_000, bytes_accessed=8_000_000, transcendentals=0
+        ),
+        name="dispatch",
+    )(rows, grads, state, first)
+
+
+def return_kernel(
+    n_sp,
+    n_tp,
+    part_ref,
+    grad_ref,
+    pick_ref,
+    mix_out,
+    pair_in,
+    far_out,
+    far_in,
+    ret_out,
+    ret_in,
+    own,
+    pair_send,
+    pair_recv,
+    far_send,
+    far_recv,
+    ret_send,
+    ret_recv,
+    mix_send,
+    mix_recv,
+):
+    at = Place(n_sp, n_tp)
+    me, t = at.me, at.t
+    width = grad_ref.shape[1]
+
+    def cols(owner):
+        return pl.ds(pl.multiple_of(owner * width, width), width)
+
+    at.enter()
+    waits = []
+    order = list(range(1, n_sp)) + [0]
+    for d in order:
+        span = at.span(d)
+        for i, partner in enumerate(at.partners()):
+            core = lax.rem(partner, at.inner)
+            for far in range(at.outer):
+                copy = remote(
+                    part_ref.at[span, :, cols(far * at.inner + core)],
+                    pair_in.at[i, far, span],
+                    pair_send.at[i, far, d],
+                    pair_recv.at[i, far, span],
+                    (me, partner),
+                )
+                copy.start()
+                waits.append(copy.wait_send)
+
+    def landed(block, sem):
+        pltpu.make_async_copy(block, block, sem).wait()
+
+    def pair_sum(span, far):
+        total = part_ref[span, :, cols(far * at.inner + at.core)].astype(F32)
+        for i in range(at.inner - 1):
+            total = total + pair_in[i, far, span].astype(F32)
+        return total
+
+    for d in order:
+        span = at.span(d)
+        for i in range(at.inner - 1):
+            for far in range(at.outer):
+                landed(pair_in.at[i, far, span], pair_recv.at[i, far, span])
+        for j in range(1, at.outer):
+            far = lax.rem(at.far + j, at.outer)
+            far_out[j - 1, span] = pair_sum(span, far).astype(BF16)
+            copy = remote(
+                far_out.at[j - 1, span],
+                far_in.at[j - 1, span],
+                far_send.at[j - 1, d],
+                far_recv.at[j - 1, span],
+                (me, far * at.inner + at.core),
+            )
+            copy.start()
+            waits.append(copy.wait_send)
+    for d in order:
+        span = at.span(d)
+        total = pair_sum(span, at.far)
+        for j in range(1, at.outer):
+            landed(far_in.at[j - 1, span], far_recv.at[j - 1, span])
+            total = total + far_in[j - 1, span].astype(F32)
+        if d == 0:
+            ret_in[me] = total.astype(BF16)
+        else:
+            ret_out[span] = total.astype(BF16)
+            copy = remote(
+                ret_out.at[span], ret_in.at[me], ret_send.at[d], ret_recv.at[me], (span, t)
+            )
+            copy.start()
+            waits.append(copy.wait_send)
+    total = grad_ref[...].astype(F32)
+    total = total + jnp.dot(pick_ref[me], ret_in[me], preferred_element_type=F32)
+    for d in range(1, n_sp):
+        span = at.span_back(d)
+        landed(ret_in.at[span], ret_recv.at[span])
+        total = total + jnp.dot(pick_ref[span], ret_in[span], preferred_element_type=F32)
+    own[...] = total.astype(BF16)
+    mix_out[:, cols(t)] = total.astype(BF16)
+    near = at.outers() + at.partners()
+    for i, peer in enumerate(near):
+        copy = remote(own, mix_out.at[:, cols(t)], mix_send.at[0, i], mix_recv.at[t], (me, peer))
+        copy.start()
+        waits.append(copy.wait_send)
+    for j, owner in enumerate(at.outers()):
+        block = mix_out.at[:, cols(owner)]
+        landed(block, mix_recv.at[owner])
+        for i, partner in enumerate(at.partners()):
+            copy = remote(
+                block, block, mix_send.at[1 + j, i], mix_recv.at[owner], (me, partner)
+            )
+            copy.start()
+            waits.append(copy.wait_send)
+    for partner in at.partners():
+        core = lax.rem(partner, at.inner)
+        for far in range(at.outer):
+            owner = far * at.inner + core
+            landed(mix_out.at[:, cols(owner)], mix_recv.at[owner])
+    for wait in waits:
+        wait()
+
+
+def return_rows(partial, grad_rows, pick, n_tp):
+    n_sp, capacity, model_width = partial.shape
+    tokens, width = grad_rows.shape
+    inner = 2 if n_tp % 2 == 0 else 1
+    outer = n_tp // inner
+    blocks = (n_sp, capacity, width)
+    return pl.pallas_call(
+        functools.partial(return_kernel, n_sp, n_tp),
+        out_shape=jax.ShapeDtypeStruct((tokens, model_width), BF16),
+        in_specs=whole(3),
+        out_specs=whole(1)[0],
+        scratch_shapes=[
+            pltpu.VMEM((max(inner - 1, 1), outer) + blocks, BF16),
+            pltpu.VMEM((max(outer - 1, 1),) + blocks, BF16),
+            pltpu.VMEM((max(outer - 1, 1),) + blocks, BF16),
+            pltpu.VMEM(blocks, BF16),
+            pltpu.VMEM(blocks, BF16),
+            pltpu.VMEM((tokens, width), BF16),
+            DMA((max(inner - 1, 1), outer, n_sp)),
+            DMA((max(inner - 1, 1), outer, n_sp)),
+            DMA((max(outer - 1, 1), n_sp)),
+            DMA((max(outer - 1, 1), n_sp)),
+            DMA((n_sp,)),
+            DMA((n_sp,)),
+            DMA((outer, n_tp)),
+            DMA((n_tp,)),
+        ],
+        compiler_params=pltpu.CompilerParams(collective_id=2, has_side_effects=True),
+        cost_estimate=pl.CostEstimate(
+            flops=20_000_000_000, bytes_accessed=8_000_000, transcendentals=0
+        ),
+        name="return_rows",
+    )(partial, grad_rows, pick)
+
+
+def after_kernel(
+    n_sp,
+    n_tp,
+    reached_ref,
+    decays_ref,
+    mix_ref,
+    later_out,
+    mix_out,
+    reached_in,
+    after_tmp,
+    reach_send,
+    reach_recv,
+    back_send,
+    back_recv,
+    mix_send,
+    mix_recv,
+    fwd_send,
+    fwd_recv,
+):
+    at = Place(n_sp, n_tp)
+    me, t = at.me, at.t
+    per = reached_ref.shape[1]
+    half = mix_ref.shape[1] // at.inner
+
+    def share(core):
+        return pl.ds(pl.multiple_of(core * half, half), half)
+
+    def landed(block, sem):
+        pltpu.make_async_copy(block, block, sem).wait()
+
+    at.enter()
+    waits = []
+    for d in range(1, n_sp):
+        peer = at.span(d)
+        copy = remote(
+            reached_ref.at[peer], reached_in.at[me], reach_send.at[d], reach_recv.at[me], (peer, t)
+        )
+        copy.start()
+        waits.append(copy.wait_send)
+    for d in range(1, n_sp):
+        peer = at.span(d)
+        copy = remote(
+            mix_ref.at[peer, share(at.core)],
+            mix_out.at[me, share(at.core)],
+            mix_send.at[d],
+            mix_recv.at[me],
+            (peer, t),
+        )
+        copy.start()
+        waits.append(copy.wait_send)
+    reached_in[me] = reached_ref[me]
+    mix_out[me] = mix_ref[me]
+    for d in range(1, n_sp):
+        src_span = at.span_back(d)
+        landed(reached_in.at[src_span], reach_recv.at[src_span])
+    running = jnp.zeros(reached_ref.shape[1:], F32)
+    for k in reversed(range(n_sp)):
+        after_tmp[k] = running.astype(BF16)
+        running = decay_column(decays_ref[k], per) * running + reached_in[k].astype(F32)
+    for d in range(1, n_sp):
+        peer = at.span(d)
+        copy = remote(
+            after_tmp.at[peer], later_out.at[me], back_send.at[d], back_recv.at[me], (peer, t)
+        )
+        copy.start()
+        waits.append(copy.wait_send)
+    later_out[me] = after_tmp[me]
+    for d in range(1, n_sp):
+        src_span = at.span_back(d)
+        block = mix_out.at[src_span, share(at.core)]
+        landed(block, mix_recv.at[src_span])
+        for i, partner in enumerate(at.partners()):
+            copy = remote(
+                block, block, fwd_send.at[i, d], fwd_recv.at[i, src_span], (me, partner)
+            )
+            copy.start()
+            waits.append(copy.wait_send)
+    for d in range(1, n_sp):
+        src_span = at.span_back(d)
+        for i, partner in enumerate(at.partners()):
+            landed(
+                mix_out.at[src_span, share(lax.rem(partner, at.inner))], fwd_recv.at[i, src_span]
+            )
+        landed(later_out.at[src_span], back_recv.at[src_span])
+    for wait in waits:
+        wait()
+
+
+def gradient_after(reached, decays, mix, n_tp):
+    n_sp = reached.shape[0]
+    inner = 2 if n_tp % 2 == 0 else 1
+    return pl.pallas_call(
+        functools.partial(after_kernel, n_sp, n_tp),
+        out_shape=(
+            jax.ShapeDtypeStruct(reached.shape, BF16),
+            jax.ShapeDtypeStruct(mix.shape, BF16),
+        ),
+        in_specs=whole(3),
+        out_specs=tuple(whole(2)),
+        scratch_shapes=[
+            pltpu.VMEM(reached.shape, BF16),
+            pltpu.VMEM(reached.shape, BF16),
+            DMA((n_sp,)),
+            DMA((n_sp,)),
+            DMA((n_sp,)),
+            DMA((n_sp,)),
+            DMA((n_sp,)),
+            DMA((n_sp,)),
+            DMA((max(inner - 1, 1), n_sp)),
+            DMA((max(inner - 1, 1), n_sp)),
+        ],
+        compiler_params=pltpu.CompilerParams(collective_id=3, has_side_effects=True),
+        cost_estimate=pl.CostEstimate(
+            flops=15_000_000_000, bytes_accessed=4_000_000, transcendentals=0
+        ),
+        name="gradient_after",
+    )(reached, decays, mix)
+
+
+def pack_state(state, decay, count):
     width = state.shape[-1]
-    rows = state.shape[0] * state.shape[1]
-    per = rows // count
+    per = state.shape[0] * state.shape[1] // count
     row_decay = jnp.repeat(decay, state.shape[1]).reshape(count, per)
     lines = -(-per // width)
     row_decay = jnp.pad(row_decay, ((0, 0), (0, lines * width - per)))
-    packed = jnp.concatenate(
+    return jnp.concatenate(
         [state.reshape(count, per, width), row_decay.reshape(count, lines, width)], axis=1
-    )
-    arrived = span_rows(packed, axis)
-    decays = arrived[:, per:].reshape(count, lines * width)[:, :per, None]
-    running = lax.dynamic_slice_in_dim(first_state.reshape(rows, width), here * per, per, 0)
-    before = []
-    for k in range(count):
-        before.append(running)
-        running = decays[k] * running + arrived[k, :per]
-    return (span_rows(jnp.stack(before), axis).reshape(state.shape), decays)
-
-
-def gradient_after(reached, decays, axis):
-    count = lax.axis_size(axis)
-    width = reached.shape[-1]
-    arrived = span_rows(reached.reshape(count, -1, width), axis)
-    running = jnp.zeros_like(arrived[0])
-    after = []
-    for k in reversed(range(count)):
-        after.append(running)
-        running = decays[k] * running + arrived[k]
-    return span_rows(jnp.stack(after[::-1]), axis).reshape(reached.shape)
+    ).astype(BF16)
 
 
 def span_local_scan(
@@ -185,13 +655,6 @@
         up_grad, w_up, contract, preferred_element_type=jnp.float32
     )
     return lax.optimization_barrier(partial_sum.astype(jnp.bfloat16)).astype(jnp.float32)
-
-
-def add_returns(grad_rows, returned, pick):
-    gathered = lax.dot_general(
-        pick, returned, (((0,), (0,)), ((), ())), preferred_element_type=jnp.float32
-    )
-    return (grad_rows.astype(jnp.float32) + gathered).astype(jnp.bfloat16)
 
 
 def body(
@@ -223,20 +686,8 @@
     sent_rows, sent_grads, pick = pack_rows(
         mixer_output_stream, layer_output_gradient, chosen, expert_combine_weight
     )
-    columns_here = sent_rows.shape[1]
-    parts = lax.all_to_all(
-        jnp.concatenate([sent_rows, sent_grads], axis=1).reshape(expert_count, capacity, -1),
-        "sp",
-        split_axis=0,
-        concat_axis=0,
-        tiled=True,
-    )
-    part_rows, part_grads = (parts[:, :, :columns_here], parts[:, :, columns_here:])
     whole_weight = lax.all_gather(mixer_output_weight, "sp", axis=1, tiled=True)
-    routed_rows, routed_grads = (
-        lax.all_gather(part_rows, "tp", axis=2, tiled=True),
-        lax.all_gather(part_grads, "tp", axis=2, tiled=True),
-    )
+    n_tp = lax.axis_size("tp")
     head_local = head_step_size.shape[1]
     group_local = state_input_vectors.shape[1] // STATE
     input_heads = head_mixer_input.astype(jnp.float32).reshape(local_tokens, head_local, HDIM)
@@ -249,9 +700,20 @@
     within_span_state, within_span_decay = span_final_state(
         input_heads, head_step_size, head_decay_rate, extra_log_decay, input_vector_groups
     )
-    incoming_state, span_decays = state_before(
-        within_span_state, within_span_decay, state_entering_span, "sp"
-    )
+    state_shape = within_span_state.shape
+    state_rows = state_shape[0] * state_shape[1]
+    per_span = state_rows // expert_count
+    first_rows = lax.dynamic_slice_in_dim(
+        state_entering_span.reshape(state_rows, STATE), lax.axis_index("sp") * per_span, per_span, 0
+    )
+    routed_rows, routed_grads, before, span_decays = dispatch(
+        sent_rows.reshape(expert_count, capacity, -1),
+        sent_grads.reshape(expert_count, capacity, -1),
+        pack_state(within_span_state, within_span_decay, expert_count),
+        first_rows,
+        n_tp,
+    )
+    incoming_state = before.astype(jnp.float32).reshape(state_shape)
 
     def forward(input_values, time_step_values, input_vector_entries, readout_entries):
         return span_local_scan(
@@ -283,28 +745,12 @@
         routed_rows, routed_grads, hidden, gate_grad, up_grad
     )
     partial_rows = row_partial(gate_grad, up_grad, w_gate, w_up)
-    partial_rows = partial_rows.astype(jnp.bfloat16)
-    arrived = (
-        lax.all_to_all(
-            partial_rows.reshape(partial_rows.shape[0], lax.axis_size("tp"), -1).swapaxes(0, 1),
-            "tp",
-            split_axis=0,
-            concat_axis=0,
-            tiled=True,
-        )
-    )
-    summed = jnp.sum(arrived.astype(jnp.float32), axis=0).astype(jnp.bfloat16)
-    returned = lax.all_to_all(
-        summed.reshape(expert_count, capacity, -1), "sp", split_axis=0, concat_axis=0, tiled=True
-    )
-    returned, whole_weight = lax.optimization_barrier((returned, whole_weight))
-    own_cols = add_returns(
-        layer_output_gradient, returned.reshape(expert_count * capacity, -1), pick
-    )
-    mix_grad = lax.all_gather(own_cols, "tp", axis=1, tiled=True)
-    mix_columns = lax.all_to_all(mix_grad, "sp", split_axis=1, concat_axis=0, tiled=True)
-    proj_grad = lax.dot_general(
-        normed_all, mix_columns, (((0,), (0,)), ((), ())), preferred_element_type=jnp.float32
+    partial_rows = partial_rows.astype(jnp.bfloat16).reshape(expert_count, capacity, model_width)
+    mix_grad = return_rows(
+        partial_rows,
+        layer_output_gradient,
+        pick.reshape(expert_count, capacity, local_tokens).swapaxes(1, 2),
+        n_tp,
     )
     columns = mix_grad
     normed_grad = lax.dot_general(
@@ -317,7 +763,17 @@
     reached_gradient = carried_weight(
         scanned_gradient, readout_groups, head_step_size, head_decay_rate, extra_log_decay
     )
-    later_grad = gradient_after(reached_gradient, span_decays, "sp")
+    later_grad, mix_columns = gradient_after(
+        reached_gradient.astype(jnp.bfloat16).reshape(before.shape),
+        span_decays,
+        mix_grad.reshape(local_tokens, expert_count, -1).swapaxes(0, 1),
+        n_tp,
+    )
+    later_grad = later_grad.astype(jnp.float32).reshape(state_shape)
+    mix_columns = mix_columns.reshape(expert_count * local_tokens, -1)
+    proj_grad = lax.dot_general(
+        normed_all, mix_columns, (((0,), (0,)), ((), ())), preferred_element_type=jnp.float32
+    )
     input_grad, step_grad, b_grad, c_grad = pull_back((scanned_gradient, later_grad))
     return (
         grad_g[None],

time: 250 us -> 213 us (0.85)
  Pallas kernels: 0 us -> 118 us
  waiting for transfers between devices: 86.8 us -> 0.7 us
  blocking collectives: 35.5 us -> 0 us
  starting transfers between devices: 26 us -> 0.08 us
  other arithmetic: 19.1 us -> 10.6 us
    pallas_call x0 -> x3, Pallas kernels: none -> 118 us  [the longest x1 56.3 us: dispatch(): pl.pallas_call(functools.partial(dispatch_kernel, n_sp, n_tp), out_shape=...]
    all_to_all x7 -> x0, waiting for transfers between devices: 68.6 us -> none  [the longest x4 28.5 us: span_rows(): lax.all_to_all(x.astype(jnp.bfloat16), axis, split_axis=0, concat_axis=0,...]
    all_to_all x1 -> x0, blocking collectives: 27.3 us -> none  [body(): lax.all_to_all(jnp.concatenate([sent_rows, sent_grads], axis=1).reshape(e...]
    all_to_all x7 -> x0, starting transfers between devices: 25.9 us -> none  [the longest x4 14.9 us: span_rows(): lax.all_to_all(x.astype(jnp.bfloat16), axis, split_axis=0, concat_axis=0,...]
    all_gather x1, waiting for transfers between devices: 16.7 us -> 0.01 us  [body(): whole_weight = lax.all_gather(mixer_output_weight, 'sp', axis=1, tiled=True)]
    unnamed x12 -> x0, other arithmetic: 9.24 us -> none
    all_gather x1 -> x0, blocking collectives: 8.27 us -> none  [body(): mix_grad = lax.all_gather(own_cols, 'tp', axis=1, tiled=True)]
    dot_general x1, matrix products: 5.13 us -> 2.08 us  [expert_hidden(): lax.dot_general(routed_grads, w_down, (((1,), (1,)), ((), ())), preferred...]
  transfers between devices with their start and end apart: 11 -> 2, of which waited for: 8 -> 0; matrix products, arithmetic and copies ran while one was open for 30% -> 35% of each run, Pallas kernels for 0% -> 56%
where the time goes in v1:
time: 213 us; the launch traced here: 212 us
  Pallas kernels  118 us (55%)
  matrix products  47.5 us (22%)
  local copies, waits for them, and re-layouts  19.5 us (9%)
  between operations  14.8 us (7%)
  other arithmetic  10.6 us (5%)
    pallas_call x1, Pallas kernels, dispatch(): pl.pallas_call(functools.partial(dispatch_kernel, n_sp, n_tp), out_shape=...  56.3 us
    pallas_call x1, Pallas kernels, return_rows(): pl.pallas_call(functools.partial(return_kernel, n_sp, n_tp), out_shape=ja...  37.4 us
    pallas_call x1, Pallas kernels, gradient_after(): pl.pallas_call(functools.partial(after_kernel, n_sp, n_tp), out_shape=(ja...  24.9 us
    unnamed x86, local copies, waits for them, and re-layouts  6.23 us
    dot_general x3, matrix products, span_local_scan(): jnp.einsum('bghls,bsghp->blghp', affinity[:, :, None] * decays, scaled, p...  5.14 us
    dot_general x1, matrix products, body(): lax.dot_general(columns, whole_weight, (((1,), (1,)), ((), ())), preferre...  4.88 us
    dot_general x1, matrix products, expert_hidden(): pre_gate = jnp.dot(routed_rows, w_gate, preferred_element_type=jnp.float32)  4.44 us
  transfers between devices with their start and end apart: 2, of which 0 were waited for; matrix products, arithmetic and copies ran while one was open for 35% of the time, Pallas kernels for 56%

profile of v1, /device:TPU:0, one launch (start us, length us, event | category | flops | bytes accessed | tf_op | source)
XLA Modules:
  0.0 211.7 jit_solution(17102517025107094199)
XLA Ops:
  9.4 1.1 copy.310
  14.5 1.0 convolution_convert_fusion
  15.5 1.0 fusion.13
  16.5 56.3 %dispatch.1 = (bf16[8,48,2048]{2,1,0:T(8,128)(2,1)}, bf16[8,48,2048]{2,1,0:T(8,128)(2,1)}, bf16[8,128,128]{2,1,0:T(8,128)(2,1)}, bf16[8,1,128]{2,1,0:T(2,128)(2,1)}) custom-call(bf16[8,48,512]{2,1,0:T(8,128)(2,1)} %bitcast.218, bf16[8,48,512]{2,1,0:T(8,128)(2,1)} %bitcast.219, bf16[8,129,128]{2,1,0:T(8,128)(2,1)} %pad_maximum_fusion.state_ref, ...), custom_call_target="tpu_custom_call" | custom-call | flops 20000000000 | bytes 8000000 | tf_op jit(solution)/shard_map/dispatch/pallas_call | solution.py:210
  72.7 1.2 convolution_bitcast_fusion.2
  74.2 1.2 fusion.15
  76.6 1.5 mul.367
  79.8 4.4 %fusion.2 = f32[384,896]{1,0:T(8,128)S(1)} fusion(bf16[384,2048]{1,0:T(8,128)(2,1)} %bitcast.232, bf16[1,2048,896]{2,1,0:T(8,128)(2,1)} %param.21), kind=kOutput, calls=%fused_computation.2 | convolution fusion | flops 1409286144 | bytes 6619136 | tf_op jit(solution)/shard_map/dot_general | solution.py:628
  84.3 1.8 fusion.6
  86.1 4.0 %convert_bitcast_fusion = bf16[1,896,2048]{2,1,0:T(8,128)(2,1)} fusion(bf16[384,2048]{1,0:T(8,128)(2,1)S(1)} %bitcast.236, f32[384,896]{1,0:T(8,128)S(1)} %fusion.6, f32[384,896]{1,0:T(8,128)S(1)} %fusion.2), kind=kOutput, calls=%fused_computation.10 | convolution fusion | flops 1413185536 | bytes 7995392 | tf_op jit(solution)/shard_map/dot_general | solution.py:647
  90.1 2.1 multiply_convert_fusion.1
  92.2 2.0 fusion
  94.2 4.1 %convert_bitcast_fusion.2 = bf16[1,2048,896]{2,1,0:T(8,128)(2,1)} fusion(bf16[384,2048]{1,0:T(8,128)(2,1)S(1)} %bitcast.234, bf16[384,896]{1,0:T(8,128)(2,1)S(1)} %get-tuple-element.142), kind=kOutput, calls=%fused_computation.12 | convolution fusion | flops 1411121152 | bytes 5931008 | tf_op jit(solution)/shard_map/dot_general | solution.py:645
  98.3 4.1 %convert_bitcast_fusion.1 = bf16[1,2048,896]{2,1,0:T(8,128)(2,1)} fusion(bf16[384,2048]{1,0:T(8,128)(2,1)S(1)} %bitcast.235, bf16[384,896]{1,0:T(8,128)(2,1)S(1)} %get-tuple-element.141), kind=kOutput, calls=%fused_computation.11 | convolution fusion | flops 1411121152 | bytes 5931008 | tf_op jit(solution)/shard_map/dot_general | solution.py:646
  102.4 3.0 %add_convert_fusion = bf16[384,2048]{1,0:T(8,128)(2,1)} fusion(f32[384,2048]{1,0:T(8,128)S(1)} %fusion, bf16[384,896]{1,0:T(8,128)(2,1)S(1)} %get-tuple-element.141, bf16[1,2048,896]{2,1,0:T(8,128)(2,1)S(1)} %copy-done.34), kind=kOutput, calls=%fused_computation.13 | convolution fusion | flops 1410859008 | bytes 9076736 | tf_op jit(solution)/shard_map/dot_general | solution.py:654
  106.9 37.4 %return_rows.1 = bf16[128,2048]{1,0:T(8,128)(2,1)} custom-call(bf16[8,48,2048]{2,1,0:T(8,128)(2,1)} %bitcast.238, bf16[128,512]{1,0:T(8,128)(2,1)} %grad_ref.1, bf16[8,128,48]{2,1,0:T(8,128)(2,1)} %fusion.53.pick_ref), custom_call_target="tpu_custom_call" | custom-call | flops 20000000000 | bytes 8000000 | tf_op jit(solution)/shard_map/return_rows/pallas_call | solution.py:365
  144.3 2.0 copy.335
  146.4 2.0 copy.336
  148.4 4.9 %fusion.95 = (f32[128,1024]{1,0:T(8,128)}, f32[128,1024]{1,0:T(8,128)}) fusion(f32[128,1024]{1,0:T(8,128)S(1)} %copy.326, bf16[128,1024]{1,0:T(8,128)(2,1)S(1)} %copy-done.1, f32[1024]{0:T(1024)S(1)} %copy-done.27, bf16[128,2048]{1,0:T(8,128)(2,1)} %return_rows.1, bf16[1024,2048]{1,0:T(8,128)(2,1)} %all-gather.5.cloned.1.call-done), kind=kOutput, calls=%fused_computation.155 | convolution fusion | flops 537919488 | bytes 6557696 | tf_op jit(solution)/shard_map/dot_general | solution.py:756
  153.3 2.3 %mul.383 = f32[128,2,512]{2,1,0:T(2,128)} reshape(f32[128,1024]{1,0:T(8,128)} %get-tuple-element.153) | data formatting | bytes 1048576 | tf_op jit(solution)/shard_map/transpose(jvp())/mul | solution.py:602
  155.5 1.3 reduce_sum.176
  158.1 1.2 fusion.31
  159.3 1.3 copy.332
  160.6 1.0 convolution_bitcast_fusion.4
  161.7 2.4 %fusion.25 = (f32[2,8,128]{2,1,0:T(8,128)}, f32[2,8,128]{2,1,0:T(8,128)}, f32[2,128,128]{2,1,0:T(8,128)S(1)}) fusion(f32[2,8,128]{2,1,0:T(8,128)S(1)} %copy-done.26, f32[2,128,128]{2,1,0:T(8,128)S(1)} %copy-done.12, pred[128,128]{1,0:T(8,128)(4,1)S(1)} %copy-done.21, f32[2,8,64,128]{3,2,1,0:T(8,128)S(1)} %bitcast.191, f32[128,2,8,64]{0,3,2,1:T(8,128)S(1)} %bitcast.197, ...), kind=kOutput, calls=%fused_computation.51 | convolution fusion | flops 103641088 | bytes 1359872 | tf_op jit(solution)/shard_map/transpose(jvp(bghls,bsghp->blghp))/dot_general | solution.py:550
  165.0 1.0 convolution_convert_fusion.1
  166.0 24.9 %gradient_after.1 = (bf16[8,128,128]{2,1,0:T(8,128)(2,1)}, bf16[8,128,256]{2,1,0:T(8,128)(2,1)}) custom-call(bf16[8,128,128]{2,1,0:T(8,128)(2,1)} %bitcast.220, bf16[8,1,128]{2,1,0:T(2,128)(2,1)} %get-tuple-element.59.decays_ref, bf16[8,128,256]{2,1,0:T(8,128)(2,1)} %bitcast.216), custom_call_target="tpu_custom_call" | custom-call | flops 15000000512 | bytes 4000000 | tf_op jit(solution)/shard_map/gradient_after/pallas_call | solution.py:485
  190.9 1.2 multiply_reduce_fusion.2
  192.6 2.0 multiply_reduce_fusion.1
  197.0 1.1 reduce_window_sum.42
  198.2 1.6 fusion.14
  201.6 3.3 %fusion.102 = f32[1024,256]{1,0:T(8,128)} fusion(bf16[1024,1024]{1,0:T(8,128)(2,1)} %all-gather.3.cloned.1.call-done, bf16[1024,256]{1,0:T(8,128)(2,1)S(1)} %bitcast.239), kind=kOutput, calls=%fused_computation.161 | convolution fusion | flops 536870912 | bytes 3670016 | tf_op jit(solution)/shard_map/dot_general | solution.py:774
  (159 shorter events, 17.3 us)
Async XLA Ops:
  7.2 5.6 %copy-start = (f32[16,64,128]{2,1,0:T(8,128)S(1)}, f32[16,64,128]{2,1,0:T(8,128)}, u32[]{:S(2)}) copy-start(f32[16,64,128]{2,1,0:T(8,128)} %param.28) | copy-start | bytes 1572868
  7.2 3.5 %copy-start.10 = (f32[128,16]{0,1:T(8,128)S(1)}, f32[128,16]{0,1:T(8,128)}, u32[]{:S(2)}) copy-start(f32[128,16]{0,1:T(8,128)} %param.25) | copy-start | bytes 24580
  7.2 3.6 %copy-start.29 = (f32[16]{0:T(128)S(1)}, f32[16]{0:T(128)}, u32[]{:S(2)}) copy-start(f32[16]{0:T(128)} %param.26) | copy-start | bytes 196
  7.2 3.7 %copy-start.24 = (f32[128,16]{0,1:T(8,128)S(1)}, f32[128,16]{0,1:T(8,128)}, u32[]{:S(2)}) copy-start(f32[128,16]{0,1:T(8,128)} %param.27) | copy-start | bytes 24580
  7.2 4.2 %copy-start.16 = (bf16[128,256]{1,0:T(8,128)(2,1)S(1)}, bf16[128,256]{1,0:T(8,128)(2,1)}, u32[]{:S(2)}) copy-start(bf16[128,256]{1,0:T(8,128)(2,1)} %param.29) | copy-start | bytes 196612
  7.2 141.2 %all-gather.5.cloned.1.call-start = ((), (), s32[]{:S(2)}) async-start(), calls=%async_computation.1 | async-start | bytes 4718592 | tf_op jit(solution)/shard_map/all_gather | solution.py:689
  8.0 3.8 %copy-start.17 = (bf16[128,256]{1,0:T(8,128)(2,1)S(1)}, bf16[128,256]{1,0:T(8,128)(2,1)}, u32[]{:S(2)}) copy-start(bf16[128,256]{1,0:T(8,128)(2,1)} %param.30) | copy-start | bytes 196612
  8.0 193.6 %all-gather.3.cloned.1.call-start = ((), (), s32[]{:S(2)}) async-start(), calls=%async_computation | async-start | bytes 2359296 | tf_op jit(solution)/shard_map/all_gather | solution.py:738
  10.6 1.9 copy-start.28
  10.6 1.9 copy-start.31
  11.3 3.1 %copy-start.14 = (bf16[128,512]{1,0:T(8,128)(2,1)S(1)}, bf16[128,512]{1,0:T(8,128)(2,1)}, u32[]{:S(2)}) copy-start(bf16[128,512]{1,0:T(8,128)(2,1)} %param.17) | copy-start | bytes 393220
  11.7 3.7 %copy-start.15 = (bf16[128,512]{1,0:T(8,128)(2,1)S(1)}, bf16[128,512]{1,0:T(8,128)(2,1)}, u32[]{:S(2)}) copy-start(bf16[128,512]{1,0:T(8,128)(2,1)} %grad_ref.1) | copy-start | bytes 393220
  12.3 61.7 %copy-start.4 = (bf16[128,2,128]{0,2,1:T(8,128)(2,1)}, bf16[128,2,128]{0,2,1:T(8,128)(2,1)S(1)}, u32[]{:S(2)}) copy-start(bf16[128,2,128]{0,2,1:T(8,128)(2,1)S(1)} %copy.346) | copy-start | bytes 196612
  12.4 61.5 %copy-start.6 = (bf16[128,2,128]{0,2,1:T(8,128)(2,1)}, bf16[128,2,128]{0,2,1:T(8,128)(2,1)S(1)}, u32[]{:S(2)}) copy-start(bf16[128,2,128]{0,2,1:T(8,128)(2,1)S(1)} %copy.347) | copy-start | bytes 196612
  12.5 61.7 %copy-start.25 = (f32[2,8,128]{2,1,0:T(8,128)}, f32[2,8,128]{2,1,0:T(8,128)S(1)}, u32[]{:S(2)}) copy-start(f32[2,8,128]{2,1,0:T(8,128)S(1)} %copy.322) | copy-start | bytes 24580
  12.8 61.4 %copy-start.20 = (pred[128,128]{1,0:T(8,128)(4,1)}, pred[128,128]{1,0:T(8,128)(4,1)S(1)}, u32[]{:S(2)}) copy-start(pred[128,128]{1,0:T(8,128)(4,1)S(1)} %iota_compare_fusion.3) | copy-start | bytes 49156
  76.6 2.3 %copy-start.27 = (f32[1024]{0:T(1024)S(1)}, f32[1024]{0:T(1024)}, u32[]{:S(2)}) copy-start(f32[1024]{0:T(1024)} %param.32) | copy-start | bytes 12292
  79.8 4.5 %copy-start.34 = (bf16[1,2048,896]{2,1,0:T(8,128)(2,1)S(1)}, bf16[1,2048,896]{2,1,0:T(8,128)(2,1)}, u32[]{:S(2)}) copy-start(bf16[1,2048,896]{2,1,0:T(8,128)(2,1)} %param.22) | copy-start | bytes 11010052
  79.8 4.5 %copy-start.35 = (bf16[8,48,2048]{2,1,0:T(8,128)(2,1)S(1)}, bf16[8,48,2048]{2,1,0:T(8,128)(2,1)}, u32[]{:S(2)}) copy-start(bf16[8,48,2048]{2,1,0:T(8,128)(2,1)} %get-tuple-element.57) | copy-start | bytes 4718596
  86.1 4.0 %copy-start.32 = (bf16[1,896,2048]{2,1,0:T(8,128)(2,1)S(1)}, bf16[1,896,2048]{2,1,0:T(8,128)(2,1)}, u32[]{:S(2)}) copy-start(bf16[1,896,2048]{2,1,0:T(8,128)(2,1)} %param.23) | copy-start | bytes 11010052
  90.1 2.1 copy-start.33
  158.1 2.5 %copy-start.2 = (bf16[8,128,128]{2,1,0:T(8,128)(2,1)S(1)}, bf16[8,128,128]{2,1,0:T(8,128)(2,1)}, u32[]{:S(2)}) copy-start(bf16[8,128,128]{2,1,0:T(8,128)(2,1)} %get-tuple-element.56) | copy-start | bytes 786436
  159.3 2.3 %copy-start.12 = (f32[2,128,128]{2,1,0:T(8,128)S(1)}, f32[2,128,128]{2,1,0:T(8,128)}, u32[]{:S(2)}) copy-start(f32[2,128,128]{2,1,0:T(8,128)} %copy-done.11) | copy-start | bytes 393220
  159.3 2.3 %copy-start.21 = (pred[128,128]{1,0:T(8,128)(4,1)S(1)}, pred[128,128]{1,0:T(8,128)(4,1)}, u32[]{:S(2)}) copy-start(pred[128,128]{1,0:T(8,128)(4,1)} %copy-done.20) | copy-start | bytes 49156
  159.3 2.4 %copy-start.26 = (f32[2,8,128]{2,1,0:T(8,128)S(1)}, f32[2,8,128]{2,1,0:T(8,128)}, u32[]{:S(2)}) copy-start(f32[2,8,128]{2,1,0:T(8,128)} %copy-done.25) | copy-start | bytes 24580
  161.7 2.4 %copy-start.7 = (bf16[128,2,128]{0,2,1:T(8,128)(2,1)S(1)}, bf16[128,2,128]{0,2,1:T(8,128)(2,1)}, u32[]{:S(2)}) copy-start(bf16[128,2,128]{0,2,1:T(8,128)(2,1)} %copy-done.6) | copy-start | bytes 196612
  161.7 3.4 %copy-start.18 = (f32[128,16]{0,1:T(8,128)S(1)}, f32[128,16]{0,1:T(8,128)}, u32[]{:S(2)}) copy-start(f32[128,16]{0,1:T(8,128)} %copy.333) | copy-start | bytes 24580
  166.0 26.4 %copy-start.5 = (bf16[128,2,128]{0,2,1:T(8,128)(2,1)S(1)}, bf16[128,2,128]{0,2,1:T(8,128)(2,1)}, u32[]{:S(2)}) copy-start(bf16[128,2,128]{0,2,1:T(8,128)(2,1)} %copy-done.4) | copy-start | bytes 196612
  190.9 4.0 %copy-start.3 = (bf16[8,128,128]{2,1,0:T(8,128)(2,1)S(1)}, bf16[8,128,128]{2,1,0:T(8,128)(2,1)}, u32[]{:S(2)}) copy-start(bf16[8,128,128]{2,1,0:T(8,128)(2,1)} %get-tuple-element.61) | copy-start | bytes 786436
  194.6 3.6 %copy-start.8 = (f32[1,128,2,8,64]{1,4,3,2,0:T(8,128)S(1)}, f32[1,128,2,8,64]{1,4,3,2,0:T(8,128)}, u32[]{:S(2)}) copy-start(f32[1,128,2,8,64]{1,4,3,2,0:T(8,128)} %get-tuple-element.156) | copy-start | bytes 1572868
  194.6 3.6 %copy-start.13 = (f32[2,128,128]{2,1,0:T(8,128)S(1)}, f32[2,128,128]{2,1,0:T(8,128)}, u32[]{:S(2)}) copy-start(f32[2,128,128]{2,1,0:T(8,128)} %copy-done.11) | copy-start | bytes 393220
  194.6 3.6 %copy-start.22 = (pred[128,128]{1,0:T(8,128)(4,1)S(1)}, pred[128,128]{1,0:T(8,128)(4,1)}, u32[]{:S(2)}) copy-start(pred[128,128]{1,0:T(8,128)(4,1)} %copy-done.20) | copy-start | bytes 49156
  (8 other events, 12.3 us)
Sparse Core Ops, SparseCore 0:
  10.1 98.4 all-gather.4
  110.7 53.8 all-gather.2

commit v2 on v1

--- a/solution.py
+++ b/solution.py
@@ -74,26 +74,19 @@
     rows_ref,
     grads_ref,
     state_ref,
-    first_ref,
     rows_out,
     grads_out,
-    before_out,
-    decays_out,
     state_in,
-    before_tmp,
     span_send,
     tp_send,
     fwd_send,
     block_recv,
     state_send,
     state_recv,
-    back_send,
-    back_recv,
 ):
     at = Place(n_sp, n_tp)
     me, t = at.me, at.t
     width = rows_ref.shape[2]
-    per = first_ref.shape[0]
 
     def cols(owner):
         return pl.ds(pl.multiple_of(owner * width, width), width)
@@ -149,25 +142,6 @@
         for a in range(2):
             landed(a, src_span, t)
         pass_on(d, [p[1].at[src_span, :, cols(t)] for p in pairs], near, t, tp_send, 0)
-
-    for d in range(1, n_sp):
-        src_span = at.span_back(d)
-        block = state_in.at[src_span]
-        pltpu.make_async_copy(block, block, state_recv.at[src_span]).wait()
-    running = first_ref[...]
-    for k in range(n_sp):
-        before_tmp[k] = running.astype(BF16)
-        line = state_in[k, per : per + 1]
-        decays_out[k] = line
-        running = decay_column(line, per) * running + state_in[k, :per].astype(F32)
-    for d in range(1, n_sp):
-        peer = at.span(d)
-        copy = remote(
-            before_tmp.at[peer], before_out.at[me], back_send.at[d], back_recv.at[me], (peer, t)
-        )
-        copy.start()
-        waits.append(copy.wait_send)
-    before_out[me] = before_tmp[me]
 
     for d in range(n_sp):
         src_span = at.span_back(d)
@@ -191,8 +165,8 @@
                     landed(a, src_span, far * at.inner + core)
     for d in range(1, n_sp):
         src_span = at.span_back(d)
-        block = before_out.at[src_span]
-        pltpu.make_async_copy(block, block, back_recv.at[src_span]).wait()
+        block = state_in.at[src_span]
+        pltpu.make_async_copy(block, block, state_recv.at[src_span]).wait()
     for wait in waits:
         wait()
 
@@ -201,40 +175,30 @@
     return [pl.BlockSpec(memory_space=pltpu.VMEM)] * count
 
 
-def dispatch(rows, grads, state, first, n_tp):
+def dispatch(rows, grads, state, n_tp):
     n_sp, capacity, width = rows.shape
-    per, lanes = first.shape
     inner = 2 if n_tp % 2 == 0 else 1
     near = n_tp // inner - 1 + inner - 1
     out = jax.ShapeDtypeStruct((n_sp, capacity, width * n_tp), BF16)
     return pl.pallas_call(
         functools.partial(dispatch_kernel, n_sp, n_tp),
-        out_shape=(
-            out,
-            out,
-            jax.ShapeDtypeStruct((n_sp, per, lanes), BF16),
-            jax.ShapeDtypeStruct((n_sp, 1, lanes), BF16),
-        ),
-        in_specs=whole(4),
-        out_specs=tuple(whole(4)),
+        out_shape=(out, out, jax.ShapeDtypeStruct(state.shape, BF16)),
+        in_specs=whole(3),
+        out_specs=tuple(whole(3)),
         scratch_shapes=[
-            pltpu.VMEM(state.shape, BF16),
-            pltpu.VMEM((n_sp, per, lanes), BF16),
             DMA((2, n_sp)),
             DMA((2, n_sp, max(near, 1))),
             DMA((2, n_sp, max((n_tp // inner - 1) * (inner - 1), 1))),
             DMA((2, n_sp, n_tp)),
             DMA((n_sp,)),
             DMA((n_sp,)),
-            DMA((n_sp,)),
-            DMA((n_sp,)),
         ],
         compiler_params=pltpu.CompilerParams(collective_id=1, has_side_effects=True),
         cost_estimate=pl.CostEstimate(
             flops=20_000_000_000, bytes_accessed=8_000_000, transcendentals=0
         ),
         name="dispatch",
-    )(rows, grads, state, first)
+    )(rows, grads, state)
 
 
 def return_kernel(
@@ -243,7 +207,12 @@
     part_ref,
     grad_ref,
     pick_ref,
+    state_ref,
+    first_ref,
     mix_out,
+    before_out,
+    decays_out,
+    before_tmp,
     pair_in,
     far_out,
     far_in,
@@ -258,10 +227,13 @@
     ret_recv,
     mix_send,
     mix_recv,
+    back_send,
+    back_recv,
 ):
     at = Place(n_sp, n_tp)
     me, t = at.me, at.t
     width = grad_ref.shape[1]
+    per = first_ref.shape[0]
 
     def cols(owner):
         return pl.ds(pl.multiple_of(owner * width, width), width)
@@ -310,6 +282,20 @@
             )
             copy.start()
             waits.append(copy.wait_send)
+    running = first_ref[...]
+    for k in range(n_sp):
+        before_tmp[k] = running.astype(BF16)
+        line = state_ref[k, per : per + 1]
+        decays_out[k] = line
+        running = decay_column(line, per) * running + state_ref[k, :per].astype(F32)
+    for d in range(1, n_sp):
+        peer = at.span(d)
+        copy = remote(
+            before_tmp.at[peer], before_out.at[me], back_send.at[d], back_recv.at[me], (peer, t)
+        )
+        copy.start()
+        waits.append(copy.wait_send)
+    before_out[me] = before_tmp[me]
     for d in order:
         span = at.span(d)
         total = pair_sum(span, at.far)
@@ -352,22 +338,31 @@
         for far in range(at.outer):
             owner = far * at.inner + core
             landed(mix_out.at[:, cols(owner)], mix_recv.at[owner])
+    for d in range(1, n_sp):
+        src_span = at.span_back(d)
+        landed(before_out.at[src_span], back_recv.at[src_span])
     for wait in waits:
         wait()
 
 
-def return_rows(partial, grad_rows, pick, n_tp):
+def return_rows(partial, grad_rows, pick, state, first, n_tp):
     n_sp, capacity, model_width = partial.shape
     tokens, width = grad_rows.shape
+    per, lanes = first.shape
     inner = 2 if n_tp % 2 == 0 else 1
     outer = n_tp // inner
     blocks = (n_sp, capacity, width)
     return pl.pallas_call(
         functools.partial(return_kernel, n_sp, n_tp),
-        out_shape=jax.ShapeDtypeStruct((tokens, model_width), BF16),
-        in_specs=whole(3),
-        out_specs=whole(1)[0],
+        out_shape=(
+            jax.ShapeDtypeStruct((tokens, model_width), BF16),
+            jax.ShapeDtypeStruct((n_sp, per, lanes), BF16),
+            jax.ShapeDtypeStruct((n_sp, 1, lanes), BF16),
+        ),
+        in_specs=whole(5),
+        out_specs=tuple(whole(3)),
         scratch_shapes=[
+            pltpu.VMEM((n_sp, per, lanes), BF16),
             pltpu.VMEM((max(inner - 1, 1), outer) + blocks, BF16),
             pltpu.VMEM((max(outer - 1, 1),) + blocks, BF16),
             pltpu.VMEM((max(outer - 1, 1),) + blocks, BF16),
@@ -382,13 +377,15 @@
             DMA((n_sp,)),
             DMA((outer, n_tp)),
             DMA((n_tp,)),
+            DMA((n_sp,)),
+            DMA((n_sp,)),
         ],
         compiler_params=pltpu.CompilerParams(collective_id=2, has_side_effects=True),
         cost_estimate=pl.CostEstimate(
             flops=20_000_000_000, bytes_accessed=8_000_000, transcendentals=0
         ),
         name="return_rows",
-    )(partial, grad_rows, pick)
+    )(partial, grad_rows, pick, state, first)
 
 
 def after_kernel(
@@ -521,53 +518,395 @@
     ).astype(BF16)
 
 
-def span_local_scan(
-    input_heads,
-    time_step,
-    decay_speed,
-    sudden_decay,
-    input_vector_groups,
-    readout_groups,
-    starting_state,
+HIGHEST = lax.Precision.HIGHEST
+
+
+def mm(x, y, xd=1, yd=0, precision=None):
+    return lax.dot_general(
+        x, y, (((xd,), (yd,)), ((), ())), precision=precision, preferred_element_type=F32
+    )
+
+
+def lower_ones(size):
+    down = lax.broadcasted_iota(jnp.int32, (size, size), 0)
+    across = lax.broadcasted_iota(jnp.int32, (size, size), 1)
+    return down >= across
+
+
+def head_ones(heads, channels):
+    down = lax.broadcasted_iota(jnp.int32, (heads, channels), 0)
+    across = lax.broadcasted_iota(jnp.int32, (heads, channels), 1)
+    return jnp.where(lax.div(across, HDIM) == down, 1.0, 0.0).astype(F32)
+
+
+def log_decay_sums(step_ref, rate_ref, extra_ref):
+    log_decay = extra_ref[...] - step_ref[...] * rate_ref[...]
+    lower = jnp.where(lower_ones(log_decay.shape[0]), 1.0, 0.0).astype(F32)
+    down = mm(lower, log_decay, precision=HIGHEST)
+    across = mm(log_decay, lower, 0, 1, precision=HIGHEST)
+    return down, across
+
+
+def head_decay(down, across, head, mask):
+    gap = down[:, head : head + 1] - across[head : head + 1, :]
+    return jnp.where(mask, jnp.exp(jnp.where(mask, gap, 0.0)), 0.0)
+
+
+def group_inverse(gated, group, width):
+    part = gated[:, group * width : (group + 1) * width]
+    return lax.rsqrt(jnp.mean(part * part, axis=1, keepdims=True) + norm_eps)
+
+
+def forward_kernel(
+    x_ref, step_ref, rate_ref, extra_ref, b_ref, c_ref, before_ref, z_ref, scale_ref, y_ref, norm_ref
 ):
-    length, head_count, head_size = input_heads.shape
-    groups, state_size = (input_vector_groups.shape[1], input_vector_groups.shape[2])
-    per_group = head_count // groups
-    block_count = length // BLK
-    log_decay_total = sudden_decay - time_step * decay_speed[None, :]
-    scaled = (input_heads * time_step[:, :, None]).reshape(
-        block_count, BLK, groups, per_group, head_size
-    )
-    log_decay_total = log_decay_total.reshape(block_count, BLK, groups, per_group)
-    b_rows = input_vector_groups.reshape(block_count, BLK, groups, state_size)
-    c_rows = readout_groups.reshape(block_count, BLK, groups, state_size)
-    cumulative = jnp.cumsum(log_decay_total, axis=1)
-    causal_mask = jnp.tril(jnp.ones((BLK, BLK), dtype=bool))
-    cum_t = jnp.moveaxis(cumulative, 1, -1)
-    gaps = cum_t[..., :, None] - cum_t[..., None, :]
-    decays = jnp.where(causal_mask, jnp.exp(jnp.where(causal_mask, gaps, 0.0)), 0.0)
-    affinity = jnp.einsum("blgn,bsgn->bgls", c_rows, b_rows, precision=exact_mode)
-    y_diag = jnp.einsum(
-        "bghls,bsghp->blghp", affinity[:, :, None] * decays, scaled, precision=exact_mode
-    )
-    to_end = jnp.exp(cumulative[:, -1:] - cumulative)
-    states = jnp.einsum(
-        "blgn,blghp->bghpn", b_rows, scaled * to_end[..., None], precision=exact_mode
-    )
-    block_decay = jnp.exp(cumulative[:, -1])
-
-    def advance(running, inputs):
-        block_state, decay_now = inputs
-        return (decay_now[..., None, None] * running + block_state, running)
-
-    first_state = starting_state.reshape(groups, per_group, head_size, state_size)
-    closing_state, incoming_state = lax.scan(advance, first_state, (states, block_decay))
-    y_off = (
-        jnp.einsum("blgn,bghpn->blghp", c_rows, incoming_state, precision=exact_mode)
-        * jnp.exp(cumulative)[..., None]
-    )
-    result_rows = (y_diag + y_off).reshape(length, head_count, head_size)
-    return (result_rows, closing_state.reshape(head_count, head_size, state_size))
+    tokens, channels = x_ref.shape
+    heads = step_ref.shape[1]
+    groups = b_ref.shape[1] // STATE
+    width = channels // groups
+    down, across = log_decay_sums(step_ref, rate_ref, extra_ref)
+    wide = head_ones(heads, channels)
+    mask = lower_ones(tokens)
+    lane = lax.broadcasted_iota(jnp.int32, (tokens, 2 * HDIM), 1)
+    scaled = (x_ref[...].astype(F32) * mm(step_ref[...], wide, precision=HIGHEST)).astype(BF16)
+    grown = jnp.exp(mm(down, wide, precision=HIGHEST))
+    for g in range(groups):
+        b_rows = b_ref[:, g * STATE : (g + 1) * STATE]
+        c_rows = c_ref[:, g * STATE : (g + 1) * STATE]
+        affinity = mm(c_rows, b_rows, 1, 1)
+        lanes = slice(g * width, (g + 1) * width)
+        off = mm(c_rows, before_ref[lanes], 1, 1) * grown[:, lanes]
+        pieces = []
+        for pair in range(width // (2 * HDIM)):
+            first = g * width + pair * 2 * HDIM
+            head = first // HDIM
+            values = scaled[:, first : first + 2 * HDIM]
+            left = mm((affinity * head_decay(down, across, head, mask)).astype(BF16), values)
+            right = mm((affinity * head_decay(down, across, head + 1, mask)).astype(BF16), values)
+            pieces.append(jnp.where(lane < HDIM, left, right))
+        y = jnp.concatenate(pieces, axis=1) + off
+        y_ref[:, lanes] = y
+        z = z_ref[:, lanes].astype(F32)
+        gated = y * (z * jax.nn.sigmoid(z))
+        inverse = group_inverse(gated, 0, width)
+        normed = gated * inverse * scale_ref[:, lanes]
+        norm_ref[lanes] = normed.T.astype(BF16)
+
+
+def scan_forward(x, step, rate, extra, b_rows, c_rows, before, gate, scale):
+    tokens, channels = x.shape
+    return pl.pallas_call(
+        forward_kernel,
+        out_shape=(
+            jax.ShapeDtypeStruct((tokens, channels), F32),
+            jax.ShapeDtypeStruct((channels, tokens), BF16),
+        ),
+        in_specs=whole(9),
+        out_specs=tuple(whole(2)),
+        cost_estimate=pl.CostEstimate(
+            flops=3_000_000_000, bytes_accessed=2_000_000, transcendentals=500_000
+        ),
+        name="scan_forward",
+    )(x, step, rate, extra, b_rows, c_rows, before, gate, scale)
+
+
+def ring_of(count):
+    return [k for k in range(0, count, 2)] + [k for k in reversed(range(1, count, 2))]
+
+
+def ring_origin(position, count):
+    position = lax.rem(position + 2 * count, count)
+    return jnp.where(2 * position < count, 2 * position, 2 * count - 1 - 2 * position)
+
+
+def ring_position(me, count):
+    half = lax.div(me, 2)
+    return jnp.where(lax.rem(me, 2) == 0, half, count - 1 - half)
+
+
+class Ring:
+    def __init__(self, block):
+        self.count = lax.axis_size("sp")
+        order = ring_of(self.count)
+        self.ahead = [(order[i], order[(i + 1) % self.count]) for i in range(self.count)]
+        self.back = [(b, a) for a, b in self.ahead]
+        self.blocks, self.shifts = [block], [0]
+        self.front = self.rear = block
+        self.steps = 0
+
+    def more(self):
+        return len(self.blocks) < self.count
+
+    def held(self):
+        return (self.front, self.rear)
+
+    def advance(self, held):
+        self.front, self.rear = held
+        if self.steps:
+            self.blocks[self.last[0]] = self.front
+            if self.last[1] is not None:
+                self.blocks[self.last[1]] = self.rear
+        else:
+            self.blocks[0] = self.front
+        if not self.more():
+            return
+        self.steps += 1
+        self.front = lax.ppermute(self.front, "sp", self.ahead)
+        self.blocks.append(self.front)
+        self.shifts.append(-self.steps)
+        self.last = [len(self.blocks) - 1, None]
+        if self.more():
+            self.rear = lax.ppermute(self.rear, "sp", self.back)
+            self.blocks.append(self.rear)
+            self.shifts.append(self.steps)
+            self.last[1] = len(self.blocks) - 1
+
+
+def turn(rings, *values):
+    held = [ring.held() for ring in rings]
+    values, held = lax.optimization_barrier((values, held))
+    for ring, now in zip(rings, held):
+        ring.advance(now)
+    return values if len(values) > 1 else values[0]
+
+
+def finish(ring, *values):
+    values = turn([ring], *values)
+    while ring.more():
+        values = turn([ring], *(values if isinstance(values, tuple) else (values,)))
+    return values
+
+
+def norm_grad_kernel(
+    n_sp,
+    shifts,
+    mix_ref,
+    y_ref,
+    z_ref,
+    scale_ref,
+    step_ref,
+    rate_ref,
+    extra_ref,
+    c_ref,
+    *rest,
+):
+    weights, (g_ref, gate_ref, reached_ref, total) = rest[:n_sp], rest[n_sp:]
+    channels = y_ref.shape[1]
+    heads = step_ref.shape[1]
+    groups = c_ref.shape[1] // STATE
+    width = channels // groups
+    position = ring_position(lax.axis_index("sp"), n_sp)
+    total[...] = mm(mix_ref[ring_origin(position, n_sp)], weights[0][...], 1, 1)
+    for shift, weight in zip(shifts[1:], weights[1:]):
+        total[...] += mm(mix_ref[ring_origin(position + shift, n_sp)], weight[...], 1, 1)
+    down, _ = log_decay_sums(step_ref, rate_ref, extra_ref)
+    grown = jnp.exp(mm(down, head_ones(heads, channels), precision=HIGHEST))
+    for g in range(groups):
+        lanes = slice(g * width, (g + 1) * width)
+        y, z = y_ref[:, lanes], z_ref[:, lanes].astype(F32)
+        gate = jax.nn.sigmoid(z)
+        silu = z * gate
+        gated = y * silu
+        inverse = group_inverse(gated, 0, width)
+        unit = gated * inverse
+        grad = total[:, lanes] * scale_ref[:, lanes]
+        grad = inverse * (grad - unit * jnp.mean(grad * unit, axis=1, keepdims=True))
+        gate_ref[:, lanes] = (grad * y * gate * (1.0 + z * (1.0 - gate))).astype(BF16)
+        scan_grad = grad * silu
+        g_ref[:, lanes] = scan_grad
+        weighted = (scan_grad * grown[:, lanes]).astype(BF16)
+        reached_ref[lanes] = mm(weighted, c_ref[:, g * STATE : (g + 1) * STATE], 0, 0).astype(BF16)
+
+
+def norm_grad(mix, y, gate, scale, step, rate, extra, c_rows, ring):
+    n_sp = mix.shape[0]
+    tokens, channels = y.shape
+    return pl.pallas_call(
+        functools.partial(norm_grad_kernel, n_sp, tuple(ring.shifts)),
+        out_shape=(
+            jax.ShapeDtypeStruct((tokens, channels), F32),
+            jax.ShapeDtypeStruct((tokens, channels), BF16),
+            jax.ShapeDtypeStruct((channels, STATE), BF16),
+        ),
+        in_specs=whole(8 + n_sp),
+        out_specs=tuple(whole(3)),
+        scratch_shapes=[pltpu.VMEM((tokens, channels), F32)],
+        cost_estimate=pl.CostEstimate(
+            flops=4_000_000_000, bytes_accessed=6_000_000, transcendentals=500_000
+        ),
+        name="norm_grad",
+    )(mix, y, gate, scale, step, rate, extra, c_rows, *ring.blocks)
+
+
+def backward_kernel(
+    x_ref,
+    step_ref,
+    rate_ref,
+    extra_ref,
+    b_ref,
+    c_ref,
+    before_ref,
+    g_ref,
+    later_ref,
+    dx_ref,
+    dstep_ref,
+    db_ref,
+    dc_ref,
+):
+    tokens, channels = x_ref.shape
+    heads = step_ref.shape[1]
+    groups = b_ref.shape[1] // STATE
+    width = channels // groups
+    down, across = log_decay_sums(step_ref, rate_ref, extra_ref)
+    wide = head_ones(heads, channels)
+    mask = lower_ones(tokens)
+    lane = lax.broadcasted_iota(jnp.int32, (tokens, 2 * HDIM), 1)
+    head_lane = lax.broadcasted_iota(jnp.int32, (tokens, heads), 1)
+    head_down = lax.broadcasted_iota(jnp.int32, (heads, tokens), 0)
+    last = down[tokens - 1 : tokens, :]
+    step_wide = mm(step_ref[...], wide, precision=HIGHEST)
+    down_wide = mm(down, wide, precision=HIGHEST)
+    grown = jnp.exp(down_wide)
+    to_end = jnp.exp(down_wide[tokens - 1 : tokens, :] - down_wide)
+    x = x_ref[...].astype(F32)
+    scaled = x * step_wide
+    scaled_low = scaled.astype(BF16)
+    sums = jnp.zeros((tokens, heads), F32)
+    column_sums = jnp.zeros((heads, tokens), F32)
+    through = []
+    ended = []
+    stepped = []
+    carried = []
+    for g in range(groups):
+        lanes = slice(g * width, (g + 1) * width)
+        states = slice(g * STATE, (g + 1) * STATE)
+        b_rows, c_rows = b_ref[:, states], c_ref[:, states]
+        affinity = mm(c_rows, b_rows, 1, 1)
+        before, later = before_ref[lanes], later_ref[lanes]
+        grad = g_ref[:, lanes]
+        grad_low = grad.astype(BF16)
+        affinity_grad = jnp.zeros((tokens, tokens), F32)
+        pieces = []
+        for pair in range(width // (2 * HDIM)):
+            start = pair * 2 * HDIM
+            values = scaled_low[:, g * width + start : g * width + start + 2 * HDIM]
+            grads = grad_low[:, start : start + 2 * HDIM]
+            halves = []
+            for side in range(2):
+                head = (g * width + start) // HDIM + side
+                decay = head_decay(down, across, head, mask)
+                own = grads * jnp.where((lane < HDIM) == (side == 0), 1.0, 0.0).astype(BF16)
+                inner = mm(own, values, 1, 1) * decay
+                affinity_grad = affinity_grad + inner
+                moved = inner * affinity
+                sums = sums + jnp.where(
+                    head_lane == head, jnp.sum(moved, axis=1, keepdims=True), 0.0
+                )
+                column_sums = column_sums + jnp.where(
+                    head_down == head, jnp.sum(moved, axis=0, keepdims=True), 0.0
+                )
+                halves.append(mm((affinity * decay).astype(BF16), grads, 0, 0))
+            pieces.append(jnp.where(lane < HDIM, halves[0], halves[1]))
+        ends = to_end[:, lanes]
+        from_later = mm(b_rows, later, 1, 1) * ends
+        scaled_grad = jnp.concatenate(pieces, axis=1) + from_later
+        off = mm(c_rows, before, 1, 1) * grown[:, lanes]
+        through.append(grad * off)
+        ended.append(scaled[:, lanes] * from_later)
+        stepped.append(scaled_grad * x[:, lanes])
+        dx_ref[:, lanes] = (scaled_grad * step_wide[:, lanes]).astype(BF16)
+        low = affinity_grad.astype(BF16)
+        dc_ref[:, states] = (
+            mm(low, b_rows) + mm((grad * grown[:, lanes]).astype(BF16), before)
+        ).astype(BF16)
+        db_ref[:, states] = (
+            mm(low, c_rows, 0, 0) + mm((scaled[:, lanes] * ends).astype(BF16), later)
+        ).astype(BF16)
+        both = jnp.sum(before.astype(F32) * later.astype(F32), axis=1, keepdims=True)
+        carried.append(both)
+    through = mm(jnp.concatenate(through, axis=1), wide, 1, 1, precision=HIGHEST)
+    ended = mm(jnp.concatenate(ended, axis=1), wide, 1, 1, precision=HIGHEST)
+    stepped = mm(jnp.concatenate(stepped, axis=1), wide, 1, 1, precision=HIGHEST)
+    both = jnp.broadcast_to(jnp.concatenate(carried, axis=0), (channels, STATE))
+    carried = mm(jnp.ones((8, STATE), F32), mm(wide, both, precision=HIGHEST), 1, 1, HIGHEST)
+    carried = carried[:1] * (1.0 / STATE) * jnp.exp(last)
+    moved = sums - column_sums.T + through - ended
+    final = jnp.sum(ended, axis=0, keepdims=True) + carried
+    lower = jnp.where(mask, 1.0, 0.0).astype(F32)
+    decay_grad = mm(lower, moved, 0, 0, precision=HIGHEST) + final
+    dstep_ref[...] = stepped - rate_ref[...] * decay_grad
+
+
+def scan_backward(x, step, rate, extra, b_rows, c_rows, before, grad, later):
+    tokens, channels = x.shape
+    return pl.pallas_call(
+        backward_kernel,
+        out_shape=(
+            jax.ShapeDtypeStruct(x.shape, BF16),
+            jax.ShapeDtypeStruct(step.shape, F32),
+            jax.ShapeDtypeStruct(b_rows.shape, BF16),
+            jax.ShapeDtypeStruct(c_rows.shape, BF16),
+        ),
+        in_specs=whole(9),
+        out_specs=tuple(whole(4)),
+        cost_estimate=pl.CostEstimate(
+            flops=5_000_000_000, bytes_accessed=3_000_000, transcendentals=500_000
+        ),
+        name="scan_backward",
+    )(x, step, rate, extra, b_rows, c_rows, before, grad, later)
+
+
+def projection_kernel(n_sp, shifts, mix_ref, *rest):
+    blocks, out_ref = rest[:n_sp], rest[n_sp]
+    position = ring_position(lax.axis_index("sp"), n_sp)
+    out_ref[...] = mm(blocks[0][...], mix_ref[ring_origin(position, n_sp)])
+    for shift, block in zip(shifts[1:], blocks[1:]):
+        out_ref[...] += mm(block[...], mix_ref[ring_origin(position + shift, n_sp)])
+
+
+def projection_grad(mix_columns, ring):
+    n_sp, _, columns = mix_columns.shape
+    channels = ring.blocks[0].shape[0]
+    return pl.pallas_call(
+        functools.partial(projection_kernel, n_sp, tuple(ring.shifts)),
+        out_shape=jax.ShapeDtypeStruct((channels, columns), F32),
+        in_specs=whole(1 + n_sp),
+        out_specs=whole(1)[0],
+        cost_estimate=pl.CostEstimate(
+            flops=3_000_000_000, bytes_accessed=3_000_000, transcendentals=0
+        ),
+        name="projection_grad",
+    )(mix_columns, *ring.blocks)
+
+
+def weight_grad_kernel(rows_ref, gate_ref, up_ref, hidden_ref, sent_ref, g_out, u_out, d_out):
+    g_out[...] = mm(rows_ref[...], gate_ref[...], 0, 0).astype(BF16)
+    u_out[...] = mm(rows_ref[...], up_ref[...], 0, 0).astype(BF16)
+    d_out[...] = mm(hidden_ref[...], sent_ref[...], 0, 0).astype(BF16)
+
+
+def expert_weight_grads(routed_rows, routed_grads, hidden, gate_grad, up_grad):
+    pairs, model_width = routed_rows.shape
+    units = hidden.shape[1]
+    tile = 256
+    across = pl.BlockSpec((pairs, tile), lambda i: (0, i))
+    fixed = pl.BlockSpec((pairs, units), lambda i: (0, 0))
+    tall = pl.BlockSpec((tile, units), lambda i: (i, 0))
+    return pl.pallas_call(
+        weight_grad_kernel,
+        grid=(model_width // tile,),
+        out_shape=(
+            jax.ShapeDtypeStruct((model_width, units), BF16),
+            jax.ShapeDtypeStruct((model_width, units), BF16),
+            jax.ShapeDtypeStruct((units, model_width), BF16),
+        ),
+        in_specs=[across, fixed, fixed, fixed, across],
+        out_specs=(tall, tall, pl.BlockSpec((units, tile), lambda i: (0, i))),
+        cost_estimate=pl.CostEstimate(
+            flops=6_000_000_000, bytes_accessed=16_000_000, transcendentals=0
+        ),
+        name="expert_weight_grads",
+    )(routed_rows, gate_grad, up_grad, hidden, routed_grads)
 
 
 def span_final_state(input_heads, time_step, decay_speed, sudden_decay, input_vector_groups):
@@ -581,25 +920,6 @@
     )
     result = jnp.einsum("tgn,tghp->ghpn", input_vector_groups, weighted, precision=exact_mode)
     return (result.reshape(head_count, head_size, -1), jnp.exp(sum_total))
-
-
-def carried_weight(scanned_gradient, readout_groups, time_step, decay_speed, sudden_decay):
-    length, head_count, head_size = scanned_gradient.shape
-    groups = readout_groups.shape[1]
-    log_decay_total = sudden_decay - time_step * decay_speed[None, :]
-    weighted = (
-        scanned_gradient * jnp.exp(jnp.cumsum(log_decay_total, axis=0))[:, :, None]
-    ).reshape(length, groups, head_count // groups, head_size)
-    result = jnp.einsum("tgn,tghp->ghpn", readout_groups, weighted, precision=exact_mode)
-    return result.reshape(head_count, head_size, -1)
-
-
-def gate_norm(scan_out, gate_vals, group_norm_scale, groups):
-    length = scan_out.shape[0]
-    gated = scan_out.reshape(length, -1) * jax.nn.silu(gate_vals)
-    grouped = gated.reshape(length, groups, -1)
-    factor = lax.rsqrt(jnp.mean(grouped * grouped, axis=-1, keepdims=True) + norm_eps)
-    return (grouped * factor).reshape(length, -1) * group_norm_scale[None, :]
 
 
 def slot_choice(route_rows, expert_count, capacity):
@@ -638,14 +958,6 @@
     ).astype(jnp.bfloat16)
     up_grad = (hidden_grad * activated).astype(jnp.bfloat16)
     return (hidden, gate_grad, up_grad)
-
-
-def expert_weight_grads(routed_rows, routed_grads, hidden, gate_grad, up_grad):
-    contract = (((0,), (0,)), ((), ()))
-    grad_g = lax.dot_general(routed_rows, gate_grad, contract, preferred_element_type=jnp.float32)
-    grad_u = lax.dot_general(routed_rows, up_grad, contract, preferred_element_type=jnp.float32)
-    grad_d = lax.dot_general(hidden, routed_grads, contract, preferred_element_type=jnp.float32)
-    return (grad_g.astype(jnp.bfloat16), grad_u.astype(jnp.bfloat16), grad_d.astype(jnp.bfloat16))
 
 
 def row_partial(gate_grad, up_grad, w_gate, w_up):
@@ -686,7 +998,6 @@
     sent_rows, sent_grads, pick = pack_rows(
         mixer_output_stream, layer_output_gradient, chosen, expert_combine_weight
     )
-    whole_weight = lax.all_gather(mixer_output_weight, "sp", axis=1, tiled=True)
     n_tp = lax.axis_size("tp")
     head_local = head_step_size.shape[1]
     group_local = state_input_vectors.shape[1] // STATE
@@ -694,97 +1005,106 @@
     input_vector_groups = state_input_vectors.astype(jnp.float32).reshape(
         local_tokens, group_local, STATE
     )
-    readout_groups = state_readout_vectors.astype(jnp.float32).reshape(
-        local_tokens, group_local, STATE
-    )
     within_span_state, within_span_decay = span_final_state(
         input_heads, head_step_size, head_decay_rate, extra_log_decay, input_vector_groups
     )
-    state_shape = within_span_state.shape
-    state_rows = state_shape[0] * state_shape[1]
+    state_rows = head_local * HDIM
     per_span = state_rows // expert_count
     first_rows = lax.dynamic_slice_in_dim(
         state_entering_span.reshape(state_rows, STATE), lax.axis_index("sp") * per_span, per_span, 0
     )
-    routed_rows, routed_grads, before, span_decays = dispatch(
+    packed_state = pack_state(within_span_state, within_span_decay, expert_count)
+    weight_ring = Ring(mixer_output_weight)
+    weight_ring.advance(weight_ring.held())
+    routed_rows, routed_grads, arrived_state = dispatch(
         sent_rows.reshape(expert_count, capacity, -1),
         sent_grads.reshape(expert_count, capacity, -1),
-        pack_state(within_span_state, within_span_decay, expert_count),
-        first_rows,
+        packed_state,
         n_tp,
     )
-    incoming_state = before.astype(jnp.float32).reshape(state_shape)
-
-    def forward(input_values, time_step_values, input_vector_entries, readout_entries):
-        return span_local_scan(
-            input_values,
-            time_step_values,
-            head_decay_rate,
-            extra_log_decay,
-            input_vector_entries,
-            readout_entries,
-            incoming_state,
-        )
-
-    (scan_out, closing_state), pull_back = jax.vjp(
-        forward, input_heads, head_step_size, input_vector_groups, readout_groups
-    )
-
-    def apply_norm(scan_vals, gate_vals):
-        return gate_norm(scan_vals, gate_vals, group_norm_scale, group_local)
-
-    normed, pull_norm = jax.vjp(apply_norm, scan_out, gate_preactivation.astype(jnp.float32))
-    normed_low = normed.astype(jnp.bfloat16)
-    normed_all = lax.all_gather(normed_low, "sp", axis=0, tiled=True)
-    routed_rows, normed_low = lax.optimization_barrier((routed_rows, normed_low))
+    routed_rows, routed_grads, arrived_state = turn(
+        [weight_ring], routed_rows, routed_grads, arrived_state
+    )
     model_width = routed_rows.shape[2]
     routed_rows = routed_rows.reshape(-1, model_width)
     routed_grads = routed_grads.reshape(-1, model_width)
     hidden, gate_grad, up_grad = expert_hidden(routed_rows, routed_grads, w_gate, w_up, w_down)
-    grad_g, grad_u, grad_d = expert_weight_grads(
-        routed_rows, routed_grads, hidden, gate_grad, up_grad
-    )
     partial_rows = row_partial(gate_grad, up_grad, w_gate, w_up)
     partial_rows = partial_rows.astype(jnp.bfloat16).reshape(expert_count, capacity, model_width)
-    mix_grad = return_rows(
+    partial_rows, arrived_state = turn([weight_ring], partial_rows, arrived_state)
+    mix_grad, before, span_decays = return_rows(
         partial_rows,
         layer_output_gradient,
         pick.reshape(expert_count, capacity, local_tokens).swapaxes(1, 2),
+        arrived_state,
+        first_rows,
         n_tp,
     )
-    columns = mix_grad
-    normed_grad = lax.dot_general(
-        columns,
-        whole_weight,
-        (((1,), (1,)), ((), ())),
-        preferred_element_type=jnp.float32,
-    )
-    scanned_gradient, gate_grad_in = pull_norm(normed_grad)
-    reached_gradient = carried_weight(
-        scanned_gradient, readout_groups, head_step_size, head_decay_rate, extra_log_decay
-    )
+    mix_grad, before, hidden, gate_grad, up_grad = turn(
+        [weight_ring], mix_grad, before, hidden, gate_grad, up_grad
+    )
+    rate = head_decay_rate[None, :]
+    scale = group_norm_scale[None, :]
+    before_rows = before.reshape(state_rows, STATE)
+    scan_out, normed = scan_forward(
+        head_mixer_input,
+        head_step_size,
+        rate,
+        extra_log_decay,
+        state_input_vectors,
+        state_readout_vectors,
+        before_rows,
+        gate_preactivation,
+        scale,
+    )
+    grad_g, grad_u, grad_d = expert_weight_grads(
+        routed_rows, routed_grads, hidden, gate_grad, up_grad
+    )
+    mix_parts = mix_grad.reshape(local_tokens, expert_count, -1).swapaxes(0, 1)
+    scan_out, normed, mix_parts, grad_d = finish(
+        weight_ring, scan_out, normed, mix_parts, grad_d
+    )
+    normed_ring = Ring(normed)
+    normed_ring.advance(normed_ring.held())
+    scan_grad, gate_grad_in, reached = norm_grad(
+        mix_parts,
+        scan_out,
+        gate_preactivation,
+        scale,
+        head_step_size,
+        rate,
+        extra_log_decay,
+        state_readout_vectors,
+        weight_ring,
+    )
+    scan_grad, reached = turn([normed_ring], scan_grad, reached)
     later_grad, mix_columns = gradient_after(
-        reached_gradient.astype(jnp.bfloat16).reshape(before.shape),
-        span_decays,
-        mix_grad.reshape(local_tokens, expert_count, -1).swapaxes(0, 1),
-        n_tp,
-    )
-    later_grad = later_grad.astype(jnp.float32).reshape(state_shape)
-    mix_columns = mix_columns.reshape(expert_count * local_tokens, -1)
-    proj_grad = lax.dot_general(
-        normed_all, mix_columns, (((0,), (0,)), ((), ())), preferred_element_type=jnp.float32
-    )
-    input_grad, step_grad, b_grad, c_grad = pull_back((scanned_gradient, later_grad))
+        reached.reshape(before.shape), span_decays, mix_parts, n_tp
+    )
+    later_grad, mix_columns = turn([normed_ring], later_grad, mix_columns)
+    input_grad, step_grad, b_grad, c_grad = scan_backward(
+        head_mixer_input,
+        head_step_size,
+        rate,
+        extra_log_decay,
+        state_input_vectors,
+        state_readout_vectors,
+        before_rows,
+        scan_grad,
+        later_grad.reshape(state_rows, STATE),
+    )
+    input_grad, mix_columns = finish(normed_ring, input_grad, mix_columns)
+    proj_grad = projection_grad(mix_columns, normed_ring)
     return (
         grad_g[None],
         grad_u[None],
         grad_d[None],
         proj_grad,
-        input_grad.reshape(local_tokens, -1).astype(jnp.bfloat16),
+        input_grad,
         step_grad,
-        b_grad.reshape(local_tokens, -1).astype(jnp.bfloat16),
-        c_grad.reshape(local_tokens, -1).astype(jnp.bfloat16),
-        gate_grad_in.astype(jnp.bfloat16),
+        b_grad,
+        c_grad,
+        gate_grad_in,
     )
 
 

time: 213 us -> 191 us (0.90)
  matrix products: 47.5 us -> 16.9 us
  starting transfers between devices: 0.08 us -> 19.2 us
  waiting for transfers between devices: 0.7 us -> 15.3 us
  between operations: 14.8 us -> 1.1 us
  local copies, waits for them, and re-layouts: 19.5 us -> 11.3 us
  other arithmetic: 10.6 us -> 3.64 us
  Pallas kernels: 118 us -> 123 us
    dot_general x16 -> x0, matrix products: 31.7 us -> none  [the longest x3 5.14 us: span_local_scan(): jnp.einsum('bghls,bsghp->blghp', affinity[:, :, None] * decays, scaled, p...]
    pallas_call x1 -> x6, Pallas kernels: 37.4 us -> 64.3 us  [the longest x1 33.4 us: return_rows(): pl.pallas_call(functools.partial(return_kernel, n_sp, n_tp), out_shape=(j...]
    pallas_call x1, Pallas kernels: 56.3 us -> 33 us  [dispatch(): pl.pallas_call(functools.partial(dispatch_kernel, n_sp, n_tp), out_shape=...]
    ppermute x0 -> x14, starting transfers between devices: none -> 19.2 us  [the longest x8 14.8 us: advance(): self.front = lax.ppermute(self.front, 'sp', self.ahead)]
    ppermute x0 -> x14, waiting for transfers between devices: none -> 15.3 us  [the longest x8 13.2 us: advance(): self.front = lax.ppermute(self.front, 'sp', self.ahead)]
    mul x5 -> x0, local copies, waits for them, and re-layouts: 5.33 us -> none  [the longest x2 2.46 us: gate_norm(): return (grouped * factor).reshape(length, -1) * group_norm_scale[None, :]]
    reduce_sum x7 -> x0, other arithmetic: 3.1 us -> none  [the longest x2 1.31 us: advance(): return (decay_now[..., None, None] * running + block_state, running)]
    convert_element_type x4 -> x0, other arithmetic: 2.19 us -> none  [the longest x1 1.23 us: body(): gate_grad_in.astype(jnp.bfloat16)]
  transfers between devices with their start and end apart: 2 -> 14, of which waited for: 0 -> 5; matrix products, arithmetic and copies ran while one was open for 35% -> 9% of each run, Pallas kernels for 56% -> 62%
where the time goes in v2:
time: 191 us; the launch traced here: 190 us
  Pallas kernels  123 us (64%)
  starting transfers between devices  19.2 us (10%)
  matrix products  16.9 us (9%)
  waiting for transfers between devices  15.3 us (8%)
  local copies, waits for them, and re-layouts  11.3 us (6%)
  other arithmetic  3.64 us (2%)
    pallas_call x1, Pallas kernels, return_rows(): pl.pallas_call(functools.partial(return_kernel, n_sp, n_tp), out_shape=(j...  33.4 us
    pallas_call x1, Pallas kernels, dispatch(): pl.pallas_call(functools.partial(dispatch_kernel, n_sp, n_tp), out_shape=...  33 us
    pallas_call x1, Pallas kernels, gradient_after(): pl.pallas_call(functools.partial(after_kernel, n_sp, n_tp), out_shape=(ja...  25.4 us
    ppermute x8, starting transfers between devices, advance(): self.front = lax.ppermute(self.front, 'sp', self.ahead)  14.8 us
    ppermute x8, waiting for transfers between devices, advance(): self.front = lax.ppermute(self.front, 'sp', self.ahead)  13.2 us
    pallas_call x1, Pallas kernels, expert_weight_grads(): pl.pallas_call(weight_grad_kernel, grid=(model_width // tile,), out_shape...  11 us
    pallas_call x1, Pallas kernels, scan_backward(): pl.pallas_call(backward_kernel, out_shape=(jax.ShapeDtypeStruct(x.shape,...  6.48 us
    unnamed x61, local copies, waits for them, and re-layouts  6.43 us
  transfers between devices with their start and end apart: 14, of which 5 were waited for; matrix products, arithmetic and copies ran while one was open for 9% of the time, Pallas kernels for 62%

profile of v2, /device:TPU:0, one launch (start us, length us, event | category | flops | bytes accessed | tf_op | source)
XLA Modules:
  0.0 190.2 jit_solution(18335267291506083452)
XLA Ops:
  0.7 3.1 %collective-permute-start = (bf16[1024,256]{1,0:T(8,128)(2,1)}, bf16[1024,256]{1,0:T(8,128)(2,1)S(1)}, u32[]{:S(2)}, u32[]{:S(2)}) collective-permute-start(bf16[1024,256]{1,0:T(8,128)(2,1)} %rest_0_.1), channel_id=1, source_target_pairs={{0,8},{8,16},{16,24},{24,28},{28,20},{20,12},{12,4},{4,0},{1,9},{9... | collective-permute-start | bytes 1572872 | tf_op jit(solution)/shard_map/ppermute | solution.py:654
  7.5 0.9 fusion.35
  8.8 1.1 copy.94
  10.2 1.0 convolution_convert_fusion
  11.4 1.0 fusion.13
  13.5 33.0 %dispatch.1 = (bf16[8,48,2048]{2,1,0:T(8,128)(2,1)}, bf16[8,48,2048]{2,1,0:T(8,128)(2,1)}, bf16[8,129,128]{2,1,0:T(8,128)(2,1)}) custom-call(bf16[8,48,512]{2,1,0:T(8,128)(2,1)} %bitcast.59, bf16[8,48,512]{2,1,0:T(8,128)(2,1)} %bitcast.60, bf16[8,129,128]{2,1,0:T(8,128)(2,1)} %pad_maximum_fusion.state_ref), custom_call_target="tpu_custom_call" | custom-call | flops 20000000000 | bytes 8000000 | tf_op jit(solution)/shard_map/dispatch/pallas_call | solution.py:183
  47.9 0.9 fusion.15.pick_ref
  48.8 4.7 %fusion.2 = f32[384,896]{1,0:T(8,128)S(1)} fusion(bf16[384,2048]{1,0:T(8,128)(2,1)} %bitcast.71, bf16[1,2048,896]{2,1,0:T(8,128)(2,1)} %param.21), kind=kOutput, calls=%fused_computation.2 | convolution fusion | flops 1409286144 | bytes 6619136 | tf_op jit(solution)/shard_map/dot_general | solution.py:948
  53.6 1.8 fusion.8
  56.1 3.0 %multiply_convert_fusion = (bf16[384,896]{1,0:T(8,128)(2,1)}, bf16[384,896]{1,0:T(8,128)(2,1)S(1)}, bf16[384,896]{1,0:T(8,128)(2,1)S(1)}) fusion(f32[384,896]{1,0:T(8,128)S(1)} %fusion.2, f32[384,896]{1,0:T(8,128)S(1)} %fusion.8, bf16[384,2048]{1,0:T(8,128)(2,1)S(1)} %bitcast.73, bf16[1,2048,896]{2,1,0:T(8,128)(2,1)S(1)} %copy-done.8), kind=kOutput, calls=%fused_computation.11 | convolution fusion | flops 1414447104 | bytes 10059776 | tf_op jit(solution)/shard_map/dot_general | solution.py:949
  59.1 1.8 fusion
  60.9 3.6 %collective-permute-start.2 = (bf16[1024,256]{1,0:T(8,128)(2,1)S(1)}, bf16[1024,256]{1,0:T(8,128)(2,1)S(1)}, u32[]{:S(2)}, u32[]{:S(2)}) collective-permute-start(bf16[1024,256]{1,0:T(8,128)(2,1)S(1)} %collective-permute-done.rest_1_), channel_id=1, source_target_pairs={{0,8},{8,16},{16,24},{24,28},{28,20},{20,12},{12,4},{4,0},{1,9},{9... | collective-permute-start | bytes 1572872 | tf_op jit(solution)/shard_map/ppermute | solution.py:654
  64.6 3.0 %add_convert_fusion = bf16[384,2048]{1,0:T(8,128)(2,1)} fusion(f32[384,2048]{1,0:T(8,128)S(1)} %fusion, bf16[384,896]{1,0:T(8,128)(2,1)S(1)} %get-tuple-element.77.up_ref, bf16[1,2048,896]{2,1,0:T(8,128)(2,1)S(1)} %copy-done.8), kind=kOutput, calls=%fused_computation.10 | convolution fusion | flops 1410859008 | bytes 9076736 | tf_op jit(solution)/shard_map/dot_general | solution.py:966
  67.5 9.0 %collective-permute-done.2.rest_3_ = bf16[1024,256]{1,0:T(8,128)(2,1)S(1)} collective-permute-done((bf16[1024,256]{1,0:T(8,128)(2,1)S(1)}, bf16[1024,256]{1,0:T(8,128)(2,1)S(1)}, u32[]{:S(2)}, u32[]{:S(2)}) %collective-permute-start.2) | collective-permute-done | bytes 524320 | tf_op jit(solution)/shard_map/ppermute | solution.py:654
  76.6 2.0 %collective-permute-done.3.rest_4_ = bf16[1024,256]{1,0:T(8,128)(2,1)S(1)} collective-permute-done((bf16[1024,256]{1,0:T(8,128)(2,1)S(1)}, bf16[1024,256]{1,0:T(8,128)(2,1)S(1)}, u32[]{:S(2)}, u32[]{:S(2)}) %collective-permute-start.3) | collective-permute-done | bytes 524320 | tf_op jit(solution)/shard_map/ppermute | solution.py:659
  78.6 3.5 %collective-permute-start.4 = (bf16[1024,256]{1,0:T(8,128)(2,1)S(1)}, bf16[1024,256]{1,0:T(8,128)(2,1)S(1)}, u32[]{:S(2)}, u32[]{:S(2)}) collective-permute-start(bf16[1024,256]{1,0:T(8,128)(2,1)S(1)} %collective-permute-done.2.rest_3_), channel_id=1, source_target_pairs={{0,8},{8,16},{16,24},{24,28},{28,20},{20,12},{12,4},{4,0},{1,9},{9... | collective-permute-start | bytes 1572872 | tf_op jit(solution)/shard_map/ppermute | solution.py:654
  82.1 33.4 %return_rows.1 = (bf16[128,2048]{1,0:T(8,128)(2,1)}, bf16[8,128,128]{2,1,0:T(8,128)(2,1)}, bf16[8,1,128]{2,1,0:T(2,128)(2,1)}) custom-call(bf16[8,48,2048]{2,1,0:T(8,128)(2,1)} %bitcast.76, bf16[128,512]{1,0:T(8,128)(2,1)} %grad_ref.1, bf16[8,128,48]{2,1,0:T(8,128)(2,1)} %fusion.15.pick_ref, bf16[8,129,128]{2,1,0:T(8,128)(2,1)} %get-tuple-element.71.state_ref, ...), custom_call_target="tpu_custom_call" | custom-call | flops 20000000000 | bytes 8000000 | tf_op jit(solution)/shard_map/return_rows/pallas_call | solution.py:355
  115.5 1.7 copy.103
  117.2 1.0 copy.104
  118.2 1.5 collective-permute-start.6
  119.8 3.8 %scan_forward.1 = (f32[128,1024]{1,0:T(8,128)}, bf16[1024,128]{1,0:T(8,128)(2,1)}) custom-call(bf16[128,1024]{1,0:T(8,128)(2,1)} %x_ref.3, f32[128,16]{1,0:T(8,128)} %copy-done.1, f32[1,16]{1,0:T(1,128)} %bitcast.63, f32[128,16]{1,0:T(8,128)} %copy.102.extra_ref, bf16[128,256]{1,0:T(8,128)(2,1)} %b_ref.3, bf16[128,256]{1,0:T(8,128)(2,1)} %c_ref.5, ...), custom_call_target="tpu_custom_call" | custom-call | flops 3000000000 | bytes 2000000 | tf_op jit(solution)/shard_map/scan_forward/pallas_call | solution.py:598
  123.6 11.0 %expert_weight_grads.1 = (bf16[2048,896]{1,0:T(8,128)(2,1)}, bf16[2048,896]{1,0:T(8,128)(2,1)}, bf16[896,2048]{1,0:T(8,128)(2,1)}) custom-call(bf16[384,2048]{1,0:T(8,128)(2,1)} %bitcast.72, bf16[384,896]{1,0:T(8,128)(2,1)} %copy-done.26, bf16[384,896]{1,0:T(8,128)(2,1)} %copy-done.27, bf16[384,896]{1,0:T(8,128)(2,1)} %get-tuple-element.78.hidden_ref, ...), custom_call_target="tpu_custom_call" | custom-call | flops 6000000000 | bytes 16000000 | tf_op jit(solution)/shard_map/expert_weight_grads/pallas_call | solution.py:895
  134.7 2.0 %collective-permute-start.8 = (bf16[1024,128]{1,0:T(8,128)(2,1)S(1)}, bf16[1024,128]{1,0:T(8,128)(2,1)S(1)}, u32[]{:S(2)}, u32[]{:S(2)}) collective-permute-start(bf16[1024,128]{1,0:T(8,128)(2,1)S(1)} %copy-done.16), channel_id=1, source_target_pairs={{8,0},{16,8},{24,16},{28,24},{20,28},{12,20},{4,12},{0,4},{9,1},{1... | collective-permute-start | bytes 786440 | tf_op jit(solution)/shard_map/ppermute | solution.py:659
  136.7 5.8 %norm_grad.1 = (f32[128,1024]{1,0:T(8,128)}, bf16[128,1024]{1,0:T(8,128)(2,1)}, bf16[1024,128]{1,0:T(8,128)(2,1)}) custom-call(bf16[8,128,256]{2,1,0:T(8,128)(2,1)} %bitcast.57, f32[128,1024]{1,0:T(8,128)} %get-tuple-element.90.y_ref, bf16[128,1024]{1,0:T(8,128)(2,1)} %z_ref.3, f32[1,1024]{1,0:T(1,128)} %bitcast.67, f32[128,16]{1,0:T(8,128)} %copy-done.1, ...), custom_call_target="tpu_custom_call" | custom-call | flops 4000000000 | bytes 6000000 | tf_op jit(solution)/shard_map/norm_grad/pallas_call | solution.py:724
  143.1 1.7 collective-permute-start.10
  145.1 25.4 %gradient_after.1 = (bf16[8,128,128]{2,1,0:T(8,128)(2,1)}, bf16[8,128,256]{2,1,0:T(8,128)(2,1)}) custom-call(bf16[8,128,128]{2,1,0:T(8,128)(2,1)} %bitcast.79, bf16[8,1,128]{2,1,0:T(2,128)(2,1)} %get-tuple-element.97.decays_ref, bf16[8,128,256]{2,1,0:T(8,128)(2,1)} %bitcast.58), custom_call_target="tpu_custom_call" | custom-call | flops 15000000512 | bytes 4000000 | tf_op jit(solution)/shard_map/gradient_after/pallas_call | solution.py:482
  170.6 1.3 collective-permute-start.11
  172.7 6.5 %scan_backward.1 = (bf16[128,1024]{1,0:T(8,128)(2,1)}, f32[128,16]{1,0:T(8,128)}, bf16[128,256]{1,0:T(8,128)(2,1)}, bf16[128,256]{1,0:T(8,128)(2,1)}) custom-call(bf16[128,1024]{1,0:T(8,128)(2,1)} %x_ref.3, f32[128,16]{1,0:T(8,128)} %copy-done.1, f32[1,16]{1,0:T(1,128)} %bitcast.65, f32[128,16]{1,0:T(8,128)} %copy.102.extra_ref, bf16[128,256]{1,0:T(8,128)(2,1)} %b_ref.3, ...), custom_call_target="tpu_custom_call" | custom-call | flops 5000000000 | bytes 3000000 | tf_op jit(solution)/shard_map/scan_backward/pallas_call | solution.py:842
  179.2 1.3 collective-permute-start.13
  180.5 1.5 copy.109
  182.0 3.6 %collective-permute-done.13.rest_7_ = bf16[1024,128]{1,0:T(8,128)(2,1)S(1)} collective-permute-done((bf16[1024,128]{1,0:T(8,128)(2,1)S(1)}, bf16[1024,128]{1,0:T(8,128)(2,1)S(1)}, u32[]{:S(2)}, u32[]{:S(2)}) %collective-permute-start.13) | collective-permute-done | bytes 262176 | tf_op jit(solution)/shard_map/ppermute | solution.py:654
  186.3 3.9 %projection_grad.1 = f32[1024,256]{1,0:T(8,128)} custom-call(bf16[8,128,256]{2,1,0:T(8,128)(2,1)} %get-tuple-element.107.mix_ref, bf16[1024,128]{1,0:T(8,128)(2,1)} %get-tuple-element.94.rest_0_, bf16[1024,128]{1,0:T(8,128)(2,1)} %copy-done.17, bf16[1024,128]{1,0:T(8,128)(2,1)} %copy-done.18, bf16[1024,128]{1,0:T(8,128)(2,1)} %copy-done.20, ...), custom_call_target="tpu_custom_call" | custom-call | flops 3000000000 | bytes 3000000 | tf_op jit(solution)/shard_map/projection_grad/pallas_call | solution.py:870
  (100 shorter events, 10.2 us)
Async XLA Ops:
  0.6 46.6 %copy-start = (f32[16,64,128]{2,1,0:T(8,128)S(1)}, f32[16,64,128]{2,1,0:T(8,128)}, u32[]{:S(2)}) copy-start(f32[16,64,128]{2,1,0:T(8,128)} %param.28) | copy-start | bytes 1572868
  0.7 9.3 %copy-start.4 = (bf16[128,256]{1,0:T(8,128)(2,1)S(1)}, bf16[128,256]{1,0:T(8,128)(2,1)}, u32[]{:S(2)}) copy-start(bf16[128,256]{1,0:T(8,128)(2,1)} %b_ref.3) | copy-start | bytes 196612
  0.7 9.5 %copy-start.2 = (bf16[128,512]{1,0:T(8,128)(2,1)S(1)}, bf16[128,512]{1,0:T(8,128)(2,1)}, u32[]{:S(2)}) copy-start(bf16[128,512]{1,0:T(8,128)(2,1)} %param.17) | copy-start | bytes 393220
  0.7 10.8 %copy-start.3 = (bf16[128,512]{1,0:T(8,128)(2,1)S(1)}, bf16[128,512]{1,0:T(8,128)(2,1)}, u32[]{:S(2)}) copy-start(bf16[128,512]{1,0:T(8,128)(2,1)} %grad_ref.1) | copy-start | bytes 393220
  0.7 48.1 %collective-permute-start = (bf16[1024,256]{1,0:T(8,128)(2,1)}, bf16[1024,256]{1,0:T(8,128)(2,1)S(1)}, u32[]{:S(2)}, u32[]{:S(2)}) collective-permute-start(bf16[1024,256]{1,0:T(8,128)(2,1)} %rest_0_.1), channel_id=1, source_target_pairs={{0,8},{8,16},{16,24},{24,28},{28,20},{20,12},{12,4},{4,0},{1,9},{9... | collective-permute-start | bytes 1572872 | tf_op jit(solution)/shard_map/ppermute | solution.py:654
  3.8 45.0 %collective-permute-start.1 = (bf16[1024,256]{1,0:T(8,128)(2,1)}, bf16[1024,256]{1,0:T(8,128)(2,1)S(1)}, u32[]{:S(2)}, u32[]{:S(2)}) collective-permute-start(bf16[1024,256]{1,0:T(8,128)(2,1)} %rest_0_.1), channel_id=1, source_target_pairs={{8,0},{16,8},{24,16},{28,24},{20,28},{12,20},{4,12},{0,4},{9,1},{1... | collective-permute-start | bytes 1572872 | tf_op jit(solution)/shard_map/ppermute | solution.py:659
  13.5 33.0 %copy-start.5 = (f32[128,16]{0,1:T(8,128)S(1)}, f32[128,16]{0,1:T(8,128)}, u32[]{:S(2)}) copy-start(f32[128,16]{0,1:T(8,128)} %param.27) | copy-start | bytes 24580
  48.8 12.1 %copy-start.9 = (bf16[1024,256]{1,0:T(8,128)(2,1)}, bf16[1024,256]{1,0:T(8,128)(2,1)S(1)}, u32[]{:S(2)}) copy-start(bf16[1024,256]{1,0:T(8,128)(2,1)S(1)} %collective-permute-done.rest_1_) | copy-start | bytes 1572868
  48.8 15.8 %copy-start.10 = (bf16[1024,256]{1,0:T(8,128)(2,1)}, bf16[1024,256]{1,0:T(8,128)(2,1)S(1)}, u32[]{:S(2)}) copy-start(bf16[1024,256]{1,0:T(8,128)(2,1)S(1)} %collective-permute-done.1.rest_2_) | copy-start | bytes 1572868
  60.9 15.6 %collective-permute-start.2 = (bf16[1024,256]{1,0:T(8,128)(2,1)S(1)}, bf16[1024,256]{1,0:T(8,128)(2,1)S(1)}, u32[]{:S(2)}, u32[]{:S(2)}) collective-permute-start(bf16[1024,256]{1,0:T(8,128)(2,1)S(1)} %collective-permute-done.rest_1_), channel_id=1, source_target_pairs={{0,8},{8,16},{16,24},{24,28},{28,20},{20,12},{12,4},{4,0},{1,9},{9... | collective-permute-start | bytes 1572872 | tf_op jit(solution)/shard_map/ppermute | solution.py:654
  64.6 14.0 %collective-permute-start.3 = (bf16[1024,256]{1,0:T(8,128)(2,1)S(1)}, bf16[1024,256]{1,0:T(8,128)(2,1)S(1)}, u32[]{:S(2)}, u32[]{:S(2)}) collective-permute-start(bf16[1024,256]{1,0:T(8,128)(2,1)S(1)} %collective-permute-done.1.rest_2_), channel_id=1, source_target_pairs={{8,0},{16,8},{24,16},{28,24},{20,28},{12,20},{4,12},{0,4},{9,1},{1... | collective-permute-start | bytes 1572872 | tf_op jit(solution)/shard_map/ppermute | solution.py:659
  76.5 38.9 %copy-start.11 = (bf16[1024,256]{1,0:T(8,128)(2,1)}, bf16[1024,256]{1,0:T(8,128)(2,1)S(1)}, u32[]{:S(2)}) copy-start(bf16[1024,256]{1,0:T(8,128)(2,1)S(1)} %collective-permute-done.2.rest_3_) | copy-start | bytes 1572868
  78.6 36.9 %copy-start.12 = (bf16[1024,256]{1,0:T(8,128)(2,1)}, bf16[1024,256]{1,0:T(8,128)(2,1)S(1)}, u32[]{:S(2)}) copy-start(bf16[1024,256]{1,0:T(8,128)(2,1)S(1)} %collective-permute-done.3.rest_4_) | copy-start | bytes 1572868
  78.6 36.9 %collective-permute-start.4 = (bf16[1024,256]{1,0:T(8,128)(2,1)S(1)}, bf16[1024,256]{1,0:T(8,128)(2,1)S(1)}, u32[]{:S(2)}, u32[]{:S(2)}) collective-permute-start(bf16[1024,256]{1,0:T(8,128)(2,1)S(1)} %collective-permute-done.2.rest_3_), channel_id=1, source_target_pairs={{0,8},{8,16},{16,24},{24,28},{28,20},{20,12},{12,4},{4,0},{1,9},{9... | collective-permute-start | bytes 1572872 | tf_op jit(solution)/shard_map/ppermute | solution.py:654
  82.1 33.5 %collective-permute-start.5 = (bf16[1024,256]{1,0:T(8,128)(2,1)S(1)}, bf16[1024,256]{1,0:T(8,128)(2,1)S(1)}, u32[]{:S(2)}, u32[]{:S(2)}) collective-permute-start(bf16[1024,256]{1,0:T(8,128)(2,1)S(1)} %collective-permute-done.3.rest_4_), channel_id=1, source_target_pairs={{8,0},{16,8},{24,16},{28,24},{20,28},{12,20},{4,12},{0,4},{9,1},{1... | collective-permute-start | bytes 1572872 | tf_op jit(solution)/shard_map/ppermute | solution.py:659
  115.5 8.1 %copy-start.13 = (bf16[1024,256]{1,0:T(8,128)(2,1)}, bf16[1024,256]{1,0:T(8,128)(2,1)S(1)}, u32[]{:S(2)}) copy-start(bf16[1024,256]{1,0:T(8,128)(2,1)S(1)} %collective-permute-done.4.rest_5_) | copy-start | bytes 1572868
  115.5 8.0 %copy-start.14 = (bf16[1024,256]{1,0:T(8,128)(2,1)}, bf16[1024,256]{1,0:T(8,128)(2,1)S(1)}, u32[]{:S(2)}) copy-start(bf16[1024,256]{1,0:T(8,128)(2,1)S(1)} %collective-permute-done.5.rest_6_) | copy-start | bytes 1572868
  118.2 16.3 %collective-permute-start.6 = (bf16[1024,256]{1,0:T(8,128)(2,1)S(1)}, bf16[1024,256]{1,0:T(8,128)(2,1)S(1)}, u32[]{:S(2)}, u32[]{:S(2)}) collective-permute-start(bf16[1024,256]{1,0:T(8,128)(2,1)S(1)} %collective-permute-done.4.rest_5_), channel_id=1, source_target_pairs={{0,8},{8,16},{16,24},{24,28},{28,20},{20,12},{12,4},{4,0},{1,9},{9... | collective-permute-start | bytes 1572872 | tf_op jit(solution)/shard_map/ppermute | solution.py:654
  123.6 11.0 %copy-start.16 = (bf16[1024,128]{1,0:T(8,128)(2,1)S(1)}, bf16[1024,128]{1,0:T(8,128)(2,1)}, u32[]{:S(2)}) copy-start(bf16[1024,128]{1,0:T(8,128)(2,1)} %get-tuple-element.94.rest_0_) | copy-start | bytes 786436
  134.6 8.4 %collective-permute-start.7 = (bf16[1024,128]{1,0:T(8,128)(2,1)S(1)}, bf16[1024,128]{1,0:T(8,128)(2,1)S(1)}, u32[]{:S(2)}, u32[]{:S(2)}) collective-permute-start(bf16[1024,128]{1,0:T(8,128)(2,1)S(1)} %copy-done.16), channel_id=1, source_target_pairs={{0,8},{8,16},{16,24},{24,28},{28,20},{20,12},{12,4},{4,0},{1,9},{9... | collective-permute-start | bytes 786440 | tf_op jit(solution)/shard_map/ppermute | solution.py:654
  134.7 8.4 %collective-permute-start.8 = (bf16[1024,128]{1,0:T(8,128)(2,1)S(1)}, bf16[1024,128]{1,0:T(8,128)(2,1)S(1)}, u32[]{:S(2)}, u32[]{:S(2)}) collective-permute-start(bf16[1024,128]{1,0:T(8,128)(2,1)S(1)} %copy-done.16), channel_id=1, source_target_pairs={{8,0},{16,8},{24,16},{28,24},{20,28},{12,20},{4,12},{0,4},{9,1},{1... | collective-permute-start | bytes 786440 | tf_op jit(solution)/shard_map/ppermute | solution.py:659
  143.0 27.5 %copy-start.17 = (bf16[1024,128]{1,0:T(8,128)(2,1)}, bf16[1024,128]{1,0:T(8,128)(2,1)S(1)}, u32[]{:S(2)}) copy-start(bf16[1024,128]{1,0:T(8,128)(2,1)S(1)} %collective-permute-done.7.rest_1_) | copy-start | bytes 786436
  143.1 27.4 %copy-start.18 = (bf16[1024,128]{1,0:T(8,128)(2,1)}, bf16[1024,128]{1,0:T(8,128)(2,1)S(1)}, u32[]{:S(2)}) copy-start(bf16[1024,128]{1,0:T(8,128)(2,1)S(1)} %collective-permute-done.8.rest_2_) | copy-start | bytes 786436
  143.1 27.5 %collective-permute-start.10 = (bf16[1024,128]{1,0:T(8,128)(2,1)S(1)}, bf16[1024,128]{1,0:T(8,128)(2,1)S(1)}, u32[]{:S(2)}, u32[]{:S(2)}) collective-permute-start(bf16[1024,128]{1,0:T(8,128)(2,1)S(1)} %collective-permute-done.8.rest_2_), channel_id=1, source_target_pairs={{8,0},{16,8},{24,16},{28,24},{20,28},{12,20},{4,12},{0,4},{9,1},{1... | collective-permute-start | bytes 786440 | tf_op jit(solution)/shard_map/ppermute | solution.py:659
  144.8 25.8 %collective-permute-start.9 = (bf16[1024,128]{1,0:T(8,128)(2,1)S(1)}, bf16[1024,128]{1,0:T(8,128)(2,1)S(1)}, u32[]{:S(2)}, u32[]{:S(2)}) collective-permute-start(bf16[1024,128]{1,0:T(8,128)(2,1)S(1)} %collective-permute-done.7.rest_1_), channel_id=1, source_target_pairs={{0,8},{8,16},{16,24},{24,28},{28,20},{20,12},{12,4},{4,0},{1,9},{9... | collective-permute-start | bytes 786440 | tf_op jit(solution)/shard_map/ppermute | solution.py:654
  170.6 8.6 %copy-start.19 = (bf16[1024,128]{1,0:T(8,128)(2,1)}, bf16[1024,128]{1,0:T(8,128)(2,1)S(1)}, u32[]{:S(2)}) copy-start(bf16[1024,128]{1,0:T(8,128)(2,1)S(1)} %collective-permute-done.10.rest_4_) | copy-start | bytes 786436
  170.6 8.6 %copy-start.20 = (bf16[1024,128]{1,0:T(8,128)(2,1)}, bf16[1024,128]{1,0:T(8,128)(2,1)S(1)}, u32[]{:S(2)}) copy-start(bf16[1024,128]{1,0:T(8,128)(2,1)S(1)} %collective-permute-done.9.rest_3_) | copy-start | bytes 786436
  170.6 8.6 %collective-permute-start.11 = (bf16[1024,128]{1,0:T(8,128)(2,1)S(1)}, bf16[1024,128]{1,0:T(8,128)(2,1)S(1)}, u32[]{:S(2)}, u32[]{:S(2)}) collective-permute-start(bf16[1024,128]{1,0:T(8,128)(2,1)S(1)} %collective-permute-done.9.rest_3_), channel_id=1, source_target_pairs={{0,8},{8,16},{16,24},{24,28},{28,20},{20,12},{12,4},{4,0},{1,9},{9... | collective-permute-start | bytes 786440 | tf_op jit(solution)/shard_map/ppermute | solution.py:654
  171.9 7.3 %collective-permute-start.12 = (bf16[1024,128]{1,0:T(8,128)(2,1)S(1)}, bf16[1024,128]{1,0:T(8,128)(2,1)S(1)}, u32[]{:S(2)}, u32[]{:S(2)}) collective-permute-start(bf16[1024,128]{1,0:T(8,128)(2,1)S(1)} %collective-permute-done.10.rest_4_), channel_id=1, source_target_pairs={{8,0},{16,8},{24,16},{28,24},{20,28},{12,20},{4,12},{0,4},{9,1},{1... | collective-permute-start | bytes 786440 | tf_op jit(solution)/shard_map/ppermute | solution.py:659
  179.2 6.5 %copy-start.21 = (bf16[1024,128]{1,0:T(8,128)(2,1)}, bf16[1024,128]{1,0:T(8,128)(2,1)S(1)}, u32[]{:S(2)}) copy-start(bf16[1024,128]{1,0:T(8,128)(2,1)S(1)} %collective-permute-done.11.rest_5_) | copy-start | bytes 786436
  179.2 6.4 %copy-start.22 = (bf16[1024,128]{1,0:T(8,128)(2,1)}, bf16[1024,128]{1,0:T(8,128)(2,1)S(1)}, u32[]{:S(2)}) copy-start(bf16[1024,128]{1,0:T(8,128)(2,1)S(1)} %collective-permute-done.12.rest_6_) | copy-start | bytes 786436
  179.2 6.4 %collective-permute-start.13 = (bf16[1024,128]{1,0:T(8,128)(2,1)S(1)}, bf16[1024,128]{1,0:T(8,128)(2,1)S(1)}, u32[]{:S(2)}, u32[]{:S(2)}) collective-permute-start(bf16[1024,128]{1,0:T(8,128)(2,1)S(1)} %collective-permute-done.11.rest_5_), channel_id=1, source_target_pairs={{0,8},{8,16},{16,24},{24,28},{28,20},{20,12},{12,4},{4,0},{1,9},{9... | collective-permute-start | bytes 786440 | tf_op jit(solution)/shard_map/ppermute | solution.py:654
  (10 other events, 33.2 us)
